TPU v7x, 32 devices: a whole 2x2x4 slice. The times are simulated.
32 devices in a mesh: ep: 4 (over y, x), tp: 8 (over z, core).
Axes of the slice: x: 2, y: 2, z: 4, core: 2. Of those that a mesh axis runs over, the one named last changes fastest.
Arguments:
- query_heads_rows: bfloat16 [2048, 2048], P('ep', 'tp'), may hold values from -9 to 9
- key_heads_rows: bfloat16 [2048, 2048], P('ep', 'tp'), may hold values from -9 to 9
- value_heads_rows: bfloat16 [2048, 2048], P('ep', 'tp'), may hold values from -6 to 6
- write_strength_logit: bfloat16 [16, 2048], P('tp', 'ep'), may hold values from -3.5 to -1
- decay_preactivation: bfloat16 [16, 2048], P('tp', 'ep'), may hold values from -5 to 5
- head_decay_logarithm: float32 [16], P('tp'), may hold values from -20 to -3
- extra_log_decay: float32 [16, 2048], P('tp', 'ep'), may hold values from -0.7 to 0
- output_weight: bfloat16 [2048, 2048], P('tp'), may hold values from -2 to 2
- second_batch_tokens: bfloat16 [4096, 2048], P(('ep', 'tp')), may hold values from -6 to 6
- expert_norm_scale: float32 [2048], replicated, may hold values from 0.1 to 1.9
- expert_choice_index: int32 [4096, 2], P(('ep', 'tp')), may hold values from 0 to 15, as said below
- group_router_weight: float32 [4096], P(('ep', 'tp')), may hold values from 0.25 to 1
- expert_logit_difference: float32 [4096], P(('ep', 'tp')), may hold values from -8 to 8
- expert_gate_weight: bfloat16 [16, 1024, 2048], P('ep', 'tp'), may hold values from -0.125 to 0.125
- expert_up_weight: bfloat16 [16, 1024, 2048], P('ep', 'tp'), may hold values from -0.125 to 0.125
- expert_down_weight: bfloat16 [16, 1024, 2048], P('ep', 'tp'), may hold values from -0.375 to 0.375
Outputs:
- mixer_output_first: bfloat16 [2048, 2048], P(('ep', 'tp'))
- expert_out: bfloat16 [4096, 2048], P(('ep', 'tp'))
Inputs may be any that keep to these rules, and one draw needn't show every extreme that they name: `expert_choice_index`: each row names two different experts of one group, the experts a * 4 to a * 4 + 3 for some a. In the rows of one device (aligned blocks of 128 rows) no expert is named more than 32 times, and in every device's rows some expert is named exactly 32 times.
All inputs are finite; a program needn't handle non-finite values.
Results may differ from a plain program's by a relative error of at most 0.018.
Values may be sent and summed in bfloat16 or wider, within the bound.
A program may use at most 128 MiB of HBM per device.

v0:
```python
import functools

import jax
import jax.numpy as jnp
from jax import lax
from jax.experimental import pallas as pl
from jax.experimental.pallas import tpu as pltpu
from jax.sharding import PartitionSpec as P

DK = 128
DV = 128
CAP = 32
RING = 4
MESH = pl.DeviceIdType.MESH
EPG = 4
TOPK = 2


precise_setting = lax.Precision.HIGHEST
norm_eps = 1e-06


def incoming(end_memory, axis):
    count, mine = (lax.axis_size(axis), lax.axis_index(axis))
    pieces = lax.all_gather(end_memory, axis)
    state = jnp.zeros(end_memory.shape[:-1] + (DV,), jnp.float32)
    for position in range(count - 1):
        end, transfer = pieces[position, ..., :DV], pieces[position, ..., DV:]
        longer = end + jnp.einsum("hij,hjv->hiv", transfer, state, precision=precise_setting)
        state = jnp.where(position < mine, longer, state)
    return state


def unit_rows(matrix):
    return matrix * lax.rsqrt(jnp.sum(matrix * matrix, axis=-1, keepdims=True) + norm_eps)


def mm(a, b, dims=((1,), (0,))):
    return lax.dot_general(
        a, b, (dims, ((), ())), precision=precise_setting, preferred_element_type=jnp.float32
    )


def delta_kernel(q_ref, k_ref, v_ref, strength_ref, decay_ref, local_ref, proj_ref, end_ref):
    heads = strength_ref.shape[0]
    chunk = DK
    chunks = q_ref.shape[0] // chunk
    rows = lax.broadcasted_iota(jnp.int32, (chunk, chunk), 0)
    cols = lax.broadcasted_iota(jnp.int32, (chunk, chunk), 1)
    within = rows >= cols
    eye = jnp.where(rows == cols, 1.0, 0.0)
    parts = []
    for h in range(heads):
        for c in range(chunks):
            at = pl.ds(c * chunk, chunk)
            q = q_ref[at, h * DK : (h + 1) * DK].astype(jnp.float32)
            k = k_ref[at, h * DK : (h + 1) * DK].astype(jnp.float32)
            v = v_ref[at, h * DV : (h + 1) * DV].astype(jnp.float32)
            q = unit_rows(q) * DK ** (-0.5)
            k = unit_rows(k)
            d_row = decay_ref[h : h + 1, c * chunk : (c + 1) * chunk]
            b_row = strength_ref[h : h + 1, c * chunk : (c + 1) * chunk]
            d_col = jnp.sum(jnp.where(rows == cols, d_row, 0.0), axis=1, keepdims=True)
            b_col = jnp.sum(jnp.where(rows == cols, b_row, 0.0), axis=1, keepdims=True)
            cum_col = jnp.sum(jnp.where(within, d_row, 0.0), axis=1, keepdims=True)
            cum_row = jnp.sum(jnp.where(rows <= cols, d_col, 0.0), axis=0, keepdims=True)
            last = cum_col[chunk - 1 : chunk, :]
            decayed = jnp.where(within, jnp.exp(jnp.where(within, cum_col - cum_row, 0.0)), 0.0)
            weighted = k * b_col
            lower = jnp.where(
                rows > cols, mm(weighted, k, ((1,), (1,))) * decayed, 0.0
            )
            scores = mm(q, k, ((1,), (1,))) * decayed
            grown = jnp.exp(cum_col)
            rhs = jnp.concatenate([v * b_col, weighted * grown], axis=1)
            parts.append([lower, scores, rhs, q * grown, k * jnp.exp(last - cum_col), jnp.exp(last)])
    inverses = [None] * len(parts)
    span = 1
    while span < chunk:
        mask = (
            (rows // (2 * span) == cols // (2 * span))
            & (rows // span % 2 == 1)
            & (cols // span % 2 == 0)
        )
        for i, part in enumerate(parts):
            edge = jnp.where(mask, part[0], 0.0)
            if span == 1:
                inverses[i] = eye - edge
            else:
                inverses[i] = inverses[i] - mm(mm(inverses[i], edge), inverses[i])
        span *= 2
    solved = [mm(inverse, part[2]) for inverse, part in zip(inverses, parts)]
    states = [
        jnp.concatenate([jnp.zeros((DK, DV), jnp.float32), eye], axis=1) for _ in range(heads)
    ]
    for c in range(chunks):
        for h in range(heads):
            _, scores, _, queries, keys, retention = parts[h * chunks + c]
            both = solved[h * chunks + c]
            fresh = jnp.concatenate([both[:, :DV], jnp.zeros((chunk, DK), jnp.float32)], axis=1)
            state = states[h]
            updates = fresh - mm(both[:, DV:], state)
            out = mm(queries, state) + mm(scores, updates)
            states[h] = state * retention + mm(keys, updates, ((0,), (0,)))
            at = pl.ds(c * chunk, chunk)
            local_ref[h, at, :] = out[:, :DV]
            proj_ref[h, at, :] = out[:, DV:]
    for h in range(heads):
        end_ref[h] = states[h]


def delta_rule(queries, keys, values, strength, decay_logarithm):
    heads, length = strength.shape
    vmem = pl.BlockSpec(memory_space=pltpu.VMEM)
    f32 = jnp.float32
    return pl.pallas_call(
        delta_kernel,
        out_shape=(
            jax.ShapeDtypeStruct((heads, length, DV), f32),
            jax.ShapeDtypeStruct((heads, length, DK), f32),
            jax.ShapeDtypeStruct((heads, DK, DV + DK), f32),
        ),
        in_specs=[vmem] * 5,
        out_specs=(vmem,) * 3,
        cost_estimate=pl.CostEstimate(
            flops=40 * heads * length * DK * DK * 6, bytes_accessed=4 * 2**20, transcendentals=0
        ),
        compiler_params=pltpu.CompilerParams(vmem_limit_bytes=40 * 2**20),
    )(queries, keys, values, strength, decay_logarithm)


def expert_kernel(x_ref, gate_ref, up_ref, down_ref, out_ref):
    experts, units, width = gate_ref.shape
    x = x_ref[:, :width]
    hidden = []
    for e in range(experts):
        gating = lax.dot_general(
            x, gate_ref[e], (((1,), (1,)), ((), ())), preferred_element_type=jnp.float32
        )
        upward = lax.dot_general(
            x, up_ref[e], (((1,), (1,)), ((), ())), preferred_element_type=jnp.float32
        )
        share = x_ref[:, width + e : width + e + 1].astype(jnp.float32) + x_ref[
            :, width + experts + e : width + experts + e + 1
        ].astype(jnp.float32)
        hidden.append((gating / (1.0 + jnp.exp(-gating)) * upward * share).astype(jnp.bfloat16))
    hidden = jnp.concatenate(hidden, axis=1)
    down = down_ref[...].reshape(experts * units, width)
    out_ref[...] = jnp.dot(hidden, down, preferred_element_type=jnp.float32).astype(jnp.bfloat16)


def expert_layer(rows, gate, up, down, tile):
    count, wide = rows.shape
    experts, units, width = gate.shape
    whole = pl.BlockSpec((experts, units, width), lambda i: (0, 0, 0))
    return pl.pallas_call(
        expert_kernel,
        grid=(count // tile,),
        out_shape=jax.ShapeDtypeStruct((count, width), jnp.bfloat16),
        in_specs=[pl.BlockSpec((tile, wide), lambda i: (i, 0)), whole, whole, whole],
        out_specs=pl.BlockSpec((tile, width), lambda i: (i, 0)),
        cost_estimate=pl.CostEstimate(
            flops=6 * count * experts * units * width,
            bytes_accessed=4 * count * width + 6 * experts * units * width,
            transcendentals=0,
        ),
        compiler_params=pltpu.CompilerParams(vmem_limit_bytes=48 * 2**20),
    )(rows, gate, up, down)


def exchange_kernel(
    ring, out_ref, spread_ref, gate_ref, up_ref, down_ref, result_ref,
    rows, part, theirs, pair, passed, landed, onward, total, back,
    local_sem, ep_sems, near_sems, far_sems, core_sems, pair_sems, half_sems, back_sems,
):
    e, t = lax.axis_index("ep"), lax.axis_index("tp")
    peers, slots, _ = out_ref.shape
    experts, units, width = gate_ref.shape
    half = width // 2
    core, z = lax.rem(t, 2), lax.div(t, 2)
    bf16, f32 = jnp.bfloat16, jnp.float32

    def at_chip(hop, same=True):
        return lax.rem(z + hop, ring) * 2 + (core if same else 1 - core)

    right, left, other = at_chip(1), at_chip(ring - 1), at_chip(0, False)

    def at_peer(j):
        return lax.rem(e + j, peers)

    barrier = pltpu.get_barrier_semaphore()
    greeted = [(at_peer(j), t) for j in range(1, peers)] + [(e, right), (e, left), (e, other)]
    for device in greeted:
        pl.semaphore_signal(barrier, inc=1, device_id=device, device_id_type=MESH)
    pl.semaphore_wait(barrier, len(greeted))

    started = []

    def send(src, dst, sems, index, device):
        copy = pltpu.make_async_remote_copy(
            src_ref=src,
            dst_ref=dst,
            send_sem=sems.at[(0,) + index],
            recv_sem=sems.at[(1,) + index],
            device_id=device,
            device_id_type=MESH,
        )
        copy.start()
        started.append(copy)

    def arrived(dst, sems, index):
        pltpu.make_async_remote_copy(
            src_ref=dst,
            dst_ref=dst,
            send_sem=sems.at[(0,) + index],
            recv_sem=sems.at[(1,) + index],
            device_id=(e, other),
            device_id_type=MESH,
        ).wait_recv()

    own = pltpu.make_async_copy(out_ref.at[e], rows.at[t, e], local_sem)
    own.start()
    for j in range(1, peers):
        target = at_peer(j)
        send(out_ref.at[target], rows.at[t, e], ep_sems, (j,), (target, t))
    sources = [lax.rem(e + peers - j, peers) for j in range(peers)]

    def piece(hop, j, same=True):
        return rows.at[at_chip(hop, same), sources[j]]

    def to_other(hop, j):
        send(piece(hop, j), piece(hop, j), core_sems, (hop, j), (e, other))

    def own_piece(j):
        if j == 0:
            own.wait()
        else:
            arrived(piece(0, j), ep_sems, (j,))
        send(piece(0, j), piece(0, j), near_sems, (0, j), (e, right))
        send(piece(0, j), piece(0, j), near_sems, (1, j), (e, left))
        to_other(0, j)

    def near_piece(j):
        arrived(piece(ring - 1, j), near_sems, (0, j))
        if j % 2 == 0:
            send(piece(ring - 1, j), piece(ring - 1, j), far_sems, (j,), (e, right))
        arrived(piece(1, j), near_sems, (1, j))
        if j % 2 == 1:
            send(piece(1, j), piece(1, j), far_sems, (j,), (e, left))
        to_other(ring - 1, j)
        to_other(1, j)

    def far_piece(j):
        arrived(piece(2, j), far_sems, (j,))
        to_other(2, j)

    def produce(hop):
        for j in range(peers):
            arrived(piece(hop, j, False), core_sems, (hop, j))

        def one(k, carry):
            which = lax.rem(core + 1 + k, 2)
            block = rows[lax.rem(z + hop, ring) * 2 + which].reshape(peers * slots, -1)
            x = block[:, :width]
            hidden = []
            for n in range(experts):
                gating = lax.dot_general(
                    x, gate_ref[n], (((1,), (1,)), ((), ())), preferred_element_type=f32
                )
                upward = lax.dot_general(
                    x, up_ref[n], (((1,), (1,)), ((), ())), preferred_element_type=f32
                )
                share = block[:, width + n : width + n + 1].astype(f32) + block[
                    :, width + experts + n : width + experts + n + 1
                ].astype(f32)
                hidden.append((gating / (1.0 + jnp.exp(-gating)) * upward * share).astype(bf16))
            hidden = jnp.concatenate(hidden, axis=1)
            down = down_ref[...].reshape(experts * units, width)
            for h in range(2):
                part[hop, k, h] = jnp.dot(
                    hidden, down[:, h * half : (h + 1) * half], preferred_element_type=f32
                ).astype(bf16)
            return carry

        lax.fori_loop(0, 2, one, 0)
        send(part.at[hop, 0], theirs.at[hop], pair_sems, (hop,), (e, other))

    def join(hop):
        arrived(theirs.at[hop], pair_sems, (hop,))
        for h in range(2):
            pair[hop, h] = (part[hop, 1, h].astype(f32) + theirs[hop, h].astype(f32)).astype(bf16)

    for j in range(peers):
        own_piece(j)
        if j >= 1:
            near_piece(j - 1)
        if j >= 2:
            far_piece(j - 2)
    produce(0)
    near_piece(peers - 1)
    join(0)
    far_piece(peers - 2)
    produce(1)
    produce(ring - 1)
    far_piece(peers - 1)
    join(1)
    send(pair.at[1, 1], landed.at[0, 1], half_sems, (0, 1), (e, right))
    join(ring - 1)
    send(pair.at[ring - 1, 0], landed.at[1, 0], half_sems, (1, 0), (e, left))
    produce(2)
    join(2)
    send(pair.at[2, 0], passed.at[0], half_sems, (2, 0), (e, right))
    send(pair.at[2, 1], passed.at[1], half_sems, (2, 1), (e, left))
    arrived(passed.at[0], half_sems, (2, 0))
    onward[0] = (pair[1, 0].astype(f32) + passed[0].astype(f32)).astype(bf16)
    send(onward.at[0], landed.at[0, 0], half_sems, (0, 0), (e, right))
    arrived(passed.at[1], half_sems, (2, 1))
    onward[1] = (pair[ring - 1, 1].astype(f32) + passed[1].astype(f32)).astype(bf16)
    send(onward.at[1], landed.at[1, 1], half_sems, (1, 1), (e, left))
    for h in range(2):
        arrived(landed.at[h, 1 - h], half_sems, (h, 1 - h))
    for h in range(2):
        arrived(landed.at[h, h], half_sems, (h, h))
        summed = pair[0, h].astype(f32) + landed[0, h].astype(f32) + landed[1, h].astype(f32)
        total[h] = summed.astype(bf16).reshape(peers, slots, half)
        for j in range(1, peers):
            target = at_peer(j)
            send(total.at[h, target], back.at[h, e], back_sems, (h, j), (target, t))
        back[h, e] = total[h, e]
    for h in range(2):
        for j in range(1, peers):
            arrived(back.at[h, sources[j]], back_sems, (h, j))
        result_ref[:, h * half : (h + 1) * half] = jnp.dot(
            spread_ref[...], back[h].reshape(peers * slots, half), preferred_element_type=f32
        ).astype(bf16)
    for copy in started:
        copy.wait_send()


def exchange(outgoing, spread, gate, up, down, ring):
    peers, slots, wide = outgoing.shape
    _, _, width = gate.shape
    count, half = peers * slots, width // 2
    bf16 = jnp.bfloat16
    vmem = pl.BlockSpec(memory_space=pltpu.VMEM)
    dma = pltpu.SemaphoreType.DMA
    experts, units, _ = gate.shape
    total_rows = 2 * ring * count
    return pl.pallas_call(
        functools.partial(exchange_kernel, ring),
        out_shape=jax.ShapeDtypeStruct((spread.shape[0], width), bf16),
        in_specs=[vmem] * 5,
        out_specs=vmem,
        scratch_shapes=[
            pltpu.VMEM((2 * ring, peers, slots, wide), bf16),
            pltpu.VMEM((ring, 2, 2, count, half), bf16),
            pltpu.VMEM((ring, 2, count, half), bf16),
            pltpu.VMEM((ring, 2, count, half), bf16),
            pltpu.VMEM((2, count, half), bf16),
            pltpu.VMEM((2, 2, count, half), bf16),
            pltpu.VMEM((2, count, half), bf16),
            pltpu.VMEM((2, peers, slots, half), bf16),
            pltpu.VMEM((2, peers, slots, half), bf16),
            dma,
            dma((2, peers)),
            dma((2, 2, peers)),
            dma((2, peers)),
            dma((2, ring, peers)),
            dma((2, ring)),
            dma((2, 3, 2)),
            dma((2, 2, peers)),
        ],
        cost_estimate=pl.CostEstimate(
            flops=60 * total_rows * experts * units * width,
            bytes_accessed=6 * experts * units * width,
            transcendentals=0,
        ),
        compiler_params=pltpu.CompilerParams(
            collective_id=0, has_side_effects=True, vmem_limit_bytes=60 * 2**20
        ),
    )(outgoing, spread, gate, up, down)


def by_tokens(normed, choice, mixing, gate, up, down, slots, after):
    ep_count = lax.axis_size("ep")
    local_experts = gate.shape[0]
    tokens, width = normed.shape
    bf16 = jnp.bfloat16
    f32 = jnp.float32
    named = choice[:, :, None] == jnp.arange(ep_count * local_experts, dtype=jnp.int32)
    share = jnp.sum(jnp.where(named, mixing[:, :, None], 0.0), axis=1)
    goes = jnp.any(named, axis=1).reshape(tokens, ep_count, local_experts).any(axis=-1)
    earlier = jnp.tril(jnp.ones((tokens, tokens), bf16), -1)
    rank = jnp.dot(earlier, goes.astype(bf16), preferred_element_type=f32)
    spread = goes[:, :, None] & (rank[:, :, None] == jnp.arange(slots, dtype=f32))
    spread = spread.astype(bf16)
    high = share.astype(bf16)
    low = (share - high.astype(f32)).astype(bf16)
    sent = jnp.einsum("tes,td->esd", spread, normed, preferred_element_type=f32).astype(bf16)
    extra = jnp.concatenate(
        [
            high.reshape(tokens, ep_count, local_experts),
            low.reshape(tokens, ep_count, local_experts),
        ],
        axis=-1,
    )
    extra = jnp.einsum("tes,tex->esx", spread, extra, preferred_element_type=f32).astype(bf16)
    pad = -extra.shape[-1] % 128
    extra = jnp.pad(extra, ((0, 0), (0, 0), (0, pad)))
    outgoing = jnp.concatenate([sent, extra], axis=-1)
    if lax.axis_size("tp") == 2 * RING and ep_count > 1:
        outgoing, after = lax.optimization_barrier((outgoing, after))
        flat = spread.reshape(tokens, ep_count * slots)
        return exchange(outgoing, flat, gate, up, down, RING), after
    arrived = lax.all_to_all(outgoing, "ep", split_axis=0, concat_axis=0, tiled=True)
    arrived = arrived.reshape(ep_count * slots, -1)
    everyone = lax.all_gather(arrived, "tp", axis=0, tiled=True)
    produced = expert_layer(everyone, gate, up, down, arrived.shape[0])
    summed = lax.psum_scatter(produced, "tp", scatter_dimension=0, tiled=True)
    returned = lax.all_to_all(
        summed.reshape(ep_count, slots, width), "ep", split_axis=0, concat_axis=0, tiled=True
    )
    combined = jnp.einsum("tes,esd->td", spread, returned, preferred_element_type=f32)
    return combined.astype(bf16), after


def by_weights(normed, expert_choice_index, mixing, gate, up, down):
    own_tokens, width_model = normed.shape
    ep_count = lax.axis_size("ep")
    local_experts = gate.shape[0]
    experts = local_experts * ep_count
    flat_ids = expert_choice_index.reshape(-1)
    one_hot = (flat_ids[:, None] == jnp.arange(experts, dtype=jnp.int32)[None, :]).astype(jnp.int32)
    slot_rank = jnp.sum((jnp.cumsum(one_hot, axis=0) - one_hot) * one_hot, axis=1)
    slot_index = flat_ids * CAP + slot_rank
    copy_token = jnp.arange(flat_ids.shape[0], dtype=jnp.int32) // TOPK
    slot_token = jnp.full((experts * CAP,), own_tokens, jnp.int32).at[slot_index].set(copy_token)
    outgoing = jnp.take(normed, slot_token, axis=0, mode="fill", fill_value=0).reshape(
        ep_count, local_experts, CAP, width_model
    )
    arrived = lax.all_to_all(outgoing, "ep", split_axis=0, concat_axis=0, tiled=True)
    gate_piece = lax.all_gather(gate, "tp", axis=1, tiled=True)
    up_piece = lax.all_gather(up, "tp", axis=1, tiled=True)
    down_piece = lax.all_gather(down, "tp", axis=1, tiled=True)
    gating = jnp.einsum("secd,efd->secf", arrived, gate_piece, preferred_element_type=jnp.float32)
    upward = jnp.einsum("secd,efd->secf", arrived, up_piece, preferred_element_type=jnp.float32)
    hidden = (jax.nn.silu(gating) * upward).astype(jnp.bfloat16)
    produced = jnp.einsum("secf,efd->secd", hidden, down_piece, preferred_element_type=jnp.float32)
    returned = lax.all_to_all(
        produced.astype(jnp.bfloat16), "ep", split_axis=0, concat_axis=0, tiled=True
    )
    flat_results = returned.reshape(experts * CAP, width_model)
    picked = (
        jnp.take(flat_results, slot_index, axis=0)
        .reshape(own_tokens, TOPK, width_model)
        .astype(jnp.float32)
    )
    return jnp.sum(mixing[..., None] * picked, axis=1).astype(jnp.bfloat16)


def shards(
    query_heads_rows,
    key_heads_rows,
    value_heads_rows,
    write_strength_logit,
    decay_preactivation,
    head_decay_logarithm,
    extra_log_decay,
    output_weight,
    second_batch_tokens,
    expert_norm_scale,
    expert_choice_index,
    group_router_weight,
    expert_logit_difference,
    expert_gate_weight,
    expert_up_weight,
    expert_down_weight,
):
    length = query_heads_rows.shape[0]
    local_heads = head_decay_logarithm.shape[0]
    strength = jax.nn.sigmoid(write_strength_logit.astype(jnp.float32))
    decay_logarithm = (
        -jnp.exp(head_decay_logarithm)[:, None]
        * jax.nn.softplus(decay_preactivation.astype(jnp.float32))
        + extra_log_decay
    )
    local_output, projection_matrix, end_memory = delta_rule(
        query_heads_rows, key_heads_rows, value_heads_rows, strength, decay_logarithm
    )
    incoming_rows = incoming(end_memory, "ep")
    attention_result = local_output + jnp.einsum(
        "hpg,hgd->hpd", projection_matrix, incoming_rows, precision=precise_setting
    )
    attn_rows = (
        attention_result.transpose(1, 0, 2)
        .reshape(length, local_heads * DV)
        .astype(jnp.bfloat16)
    )
    product = jnp.dot(attn_rows, output_weight, preferred_element_type=jnp.float32)
    product = product.astype(jnp.bfloat16)
    widened = second_batch_tokens.astype(jnp.float32)
    normed = (
        widened
        * lax.rsqrt(jnp.mean(widened * widened, axis=-1, keepdims=True) + norm_eps)
        * expert_norm_scale
    ).astype(jnp.bfloat16)
    leading = jax.nn.sigmoid(expert_logit_difference)
    mixing = group_router_weight[:, None] * jnp.stack([leading, 1.0 - leading], axis=-1)
    local_experts, local_units, _ = expert_gate_weight.shape
    own_tokens = second_batch_tokens.shape[0]
    ep_count, tp_count = lax.axis_size("ep"), lax.axis_size("tp")
    named_both = TOPK if local_experts % EPG == 0 else 1
    slots = min(own_tokens, local_experts * CAP // named_both)
    weights = (expert_gate_weight, expert_up_weight, expert_down_weight)
    if 2 * tp_count * ep_count * slots < 3 * local_experts * local_units * tp_count:
        expert_out, product = by_tokens(
            normed, expert_choice_index, mixing, *weights, slots, product
        )
    else:
        expert_out = by_weights(normed, expert_choice_index, mixing, *weights)
    summed = lax.psum_scatter(product, "tp", scatter_dimension=0, tiled=True)
    return (summed, expert_out)


def solution(mesh):
    in_specs = (
        P("ep", "tp"),
        P("ep", "tp"),
        P("ep", "tp"),
        P("tp", "ep"),
        P("tp", "ep"),
        P("tp"),
        P("tp", "ep"),
        P("tp", None),
        P(("ep", "tp"), None),
        P(),
        P(("ep", "tp"), None),
        P(("ep", "tp")),
        P(("ep", "tp")),
        P("ep", "tp", None),
        P("ep", "tp", None),
        P("ep", "tp", None),
    )
    out_specs = (P(("ep", "tp"), None), P(("ep", "tp"), None))
    return jax.shard_map(shards, mesh=mesh, in_specs=in_specs, out_specs=out_specs, check_vma=False)
```

profile of v0, /device:TPU:0, one launch (start us, length us, event | category | flops | bytes accessed | tf_op | source)
XLA Modules:
  0.0 253.0 jit_solution(12986508239495365747)
XLA Ops:
  7.2 0.0 copy-start
  7.2 0.0 all-gather.3.cloned.1.call-start
  7.2 0.7 exponential_negate_fusion
  8.0 0.8 fusion.37
  8.8 1.0 copy-done.1
  9.7 0.9 copy-done.2
  10.7 0.9 copy-done.3
  11.6 0.0 copy-start.5
  11.6 13.2 %shard_map.167 = (f32[2,512,128]{2,1,0:T(8,128)S(1)}, f32[2,512,128]{2,1,0:T(8,128)S(1)}, f32[2,128,256]{2,1,0:T(8,128)}) custom-call(bf16[512,256]{1,0:T(8,128)(2,1)S(1)} %copy-done.1, bf16[512,256]{1,0:T(8,128)(2,1)S(1)} %copy-done.2, bf16[512,256]{1,0:T(8,128)(2,1)S(1)} %copy-done.3, f32[2,512]{1,0:T(2,128)S(1)} %get-tuple-element.17.strength_ref, ...), custom_call_target="tpu_custom_call" | custom-call | flops 4026531840 | bytes 4194304 | tf_op jit(solution)/shard_map/pallas_call | solution.py:116
  24.8 0.0 all-gather.3.cloned.1.call-update
  24.8 0.2 reduce-scatter.2.cloned.1.call-start
  25.2 0.2 fusion.23
  25.4 0.2 convolution_convert_fusion.2
  25.5 0.1 copy.47
  25.7 0.1 copy.52
  25.9 0.1 copy.51
  26.0 0.1 eq.45
  26.1 0.2 fusion.7
  26.3 0.7 and_convert_fusion.spread_ref
  26.9 0.5 convolution_convert_fusion.1
  27.4 1.1 fusion.6.out_ref
  28.6 25.6 %all-gather.3.cloned.1.call-done = f32[8,128,256]{2,1,0:T(8,128)} async-done(((f32[2,128,256]{2,1,0:T(8,128)}), f32[8,128,256]{2,1,0:T(8,128)}) %all-gather.3.cloned.1.call-update) | async-done | bytes 1048592 | tf_op jit(solution)/shard_map/all_gather | solution.py:25
  54.2 1.2 fusion.5
  55.4 1.2 fusion.4
  56.7 1.2 fusion.3
  57.9 0.6 fusion.2
  58.5 0.1 copy.50
  58.7 2.1 convolution_convert_fusion
  60.7 0.0 reduce-scatter.2.cloned.1.call-update
  60.7 183.5 %shard_map.168 = bf16[128,2048]{1,0:T(8,128)(2,1)} custom-call(bf16[4,64,2176]{2,1,0:T(8,128)(2,1)} %fusion.6.out_ref, bf16[128,256]{1,0:T(8,128)(2,1)} %and_convert_fusion.spread_ref, bf16[4,128,2048]{2,1,0:T(8,128)(2,1)} %gate_ref.1, bf16[4,128,2048]{2,1,0:T(8,128)(2,1)} %up_ref.1, bf16[4,128,2048]{2,1,0:T(8,128)(2,1)} %down_ref.1), custom_call_target="tpu_custom_call" | custom-call | flops 128849018880 | bytes 6291456 | tf_op jit(solution)/shard_map/pallas_call | solution.py:349
  244.3 0.0 reduce-scatter.2.cloned.1.call-done
  244.3 1.9 copy.56
  (24 shorter events, 0.1 us)
Async XLA Ops:
  7.2 51.5 %copy-start = (bf16[256,2048]{1,0:T(8,128)(2,1)S(1)}, bf16[256,2048]{1,0:T(8,128)(2,1)}, u32[]{:S(2)}) copy-start(bf16[256,2048]{1,0:T(8,128)(2,1)} %param.23) | copy-start | bytes 3145732
  7.2 47.0 %all-gather.3.cloned.1.call-start = ((), (), s32[]{:S(2)}) async-start(), calls=%async_computation.2 | async-start | bytes 1310720 | tf_op jit(solution)/shard_map/all_gather | solution.py:25
  8.7 1.0 copy-start.1
  9.7 0.9 copy-start.2
  10.7 0.9 copy-start.3
  11.6 13.4 %copy-start.6 = (s32[128,2]{0,1:T(2,128)S(1)}, s32[128,2]{0,1:T(2,128)}, u32[]{:S(2)}) copy-start(s32[128,2]{0,1:T(2,128)} %param.26) | copy-start | bytes 3076
  11.6 13.5 %copy-start.8 = (f32[128]{0:T(128)S(1)}, f32[128]{0:T(128)}, u32[]{:S(2)}) copy-start(f32[128]{0:T(128)} %param.28) | copy-start | bytes 1540
  11.6 13.5 %copy-start.7 = (f32[128]{0:T(128)S(1)}, f32[128]{0:T(128)}, u32[]{:S(2)}) copy-start(f32[128]{0:T(128)} %param.27) | copy-start | bytes 1540
  11.6 14.4 %copy-start.4 = (bf16[128,2048]{1,0:T(8,128)(2,1)S(1)}, bf16[128,2048]{1,0:T(8,128)(2,1)}, u32[]{:S(2)}) copy-start(bf16[128,2048]{1,0:T(8,128)(2,1)} %param.24) | copy-start | bytes 1572868
  11.6 15.3 %copy-start.5 = (f32[2048]{0:T(1024)S(1)}, f32[2048]{0:T(1024)}, u32[]{:S(2)}) copy-start(f32[2048]{0:T(1024)} %param.25) | copy-start | bytes 24580
  24.8 219.5 %reduce-scatter.2.cloned.1.call-start = ((), (), s32[]{:S(2)}) async-start(), calls=%async_computation.1 | async-start | bytes 2359296 | tf_op jit(solution)/shard_map/reduce_scatter | solution.py:521
Sparse Core Ops, SparseCore 0:
  24.9 29.2 all-gather.2
  60.9 69.1 reduce-scatter.1
where the time goes:
time: 253 us
  Pallas kernels  197 us (78%)
  waiting for transfers between devices  25.7 us (10%)
  between operations  14.2 us (6%)
  matrix products  7.24 us (3%)
  local copies, waits for them, and re-layouts  5.37 us (2%)
  other arithmetic  3.56 us (1%)
    pallas_call x1, Pallas kernels, exchange(): pl.pallas_call(functools.partial(exchange_kernel, ring), out_shape=jax.Sh...  184 us
    all_gather x1, waiting for transfers between devices, incoming(): pieces = lax.all_gather(end_memory, axis)  25.6 us
    pallas_call x1, Pallas kernels, delta_rule(): pl.pallas_call(delta_kernel, out_shape=(jax.ShapeDtypeStruct((heads, leng...  13.2 us
  transfers between devices with their start and end apart: 2, of which 1 were waited for; matrix products, arithmetic and copies ran while one was open for 1% of the time, Pallas kernels for 73%

commit v1 on v0

--- a/solution.py
+++ b/solution.py
@@ -41,7 +41,7 @@
     )
 
 
-def delta_kernel(q_ref, k_ref, v_ref, strength_ref, decay_ref, local_ref, proj_ref, end_ref):
+def delta_body(q_ref, k_ref, v_ref, strength_ref, decay_ref, local_ref, proj_ref, end_ref):
     heads = strength_ref.shape[0]
     chunk = DK
     chunks = q_ref.shape[0] // chunk
@@ -106,7 +106,7 @@
             local_ref[h, at, :] = out[:, :DV]
             proj_ref[h, at, :] = out[:, DV:]
     for h in range(heads):
-        end_ref[h] = states[h]
+        end_ref[h] = states[h].astype(end_ref.dtype)
 
 
 def delta_rule(queries, keys, values, strength, decay_logarithm):
@@ -114,7 +114,7 @@
     vmem = pl.BlockSpec(memory_space=pltpu.VMEM)
     f32 = jnp.float32
     return pl.pallas_call(
-        delta_kernel,
+        delta_body,
         out_shape=(
             jax.ShapeDtypeStruct((heads, length, DV), f32),
             jax.ShapeDtypeStruct((heads, length, DK), f32),
@@ -168,217 +168,469 @@
     )(rows, gate, up, down)
 
 
-def exchange_kernel(
-    ring, out_ref, spread_ref, gate_ref, up_ref, down_ref, result_ref,
-    rows, part, theirs, pair, passed, landed, onward, total, back,
-    local_sem, ep_sems, near_sems, far_sems, core_sems, pair_sems, half_sems, back_sems,
+def fused_kernel(
+    q_hbm, k_hbm, v_hbm, strength_ref, decay_ref, wout_hbm, tokens_hbm, scale_ref, info_ref,
+    gate_hbm, up_hbm, down_hbm, mixed_ref, expert_ref,
+    q_ref, k_ref, v_ref, wout_ref, tokens_ref, gate_ref, up_ref, down_ref,
+    raw, infos, spreads, stage, stage_share, rows, rows_share, hid, res, theirs, back,
+    acc, inb, local, proj, attn, states_out, states_in, state, prod, prod_theirs, mixed_in,
+    load_sems, ag_s, ag_r, agi_s, agi_r, ep_s, ep_r, eps_s, eps_r, core_s, core_r, cores_s, cores_r,
+    pair_s, pair_r, back_s, back_r, rs_s, rs_r, st_s, st_r, pp_s, pp_r, mr_s, mr_r,
 ):
     e, t = lax.axis_index("ep"), lax.axis_index("tp")
-    peers, slots, _ = out_ref.shape
-    experts, units, width = gate_ref.shape
-    half = width // 2
     core, z = lax.rem(t, 2), lax.div(t, 2)
+    chips, tokens, width = raw.shape
+    peers, slots = stage.shape[1], stage.shape[2]
+    experts, units, _ = gate_ref.shape
+    count = peers * slots
+    halves, half = acc.shape[1], acc.shape[3]
+    last = chips - 1
     bf16, f32 = jnp.bfloat16, jnp.float32
-
-    def at_chip(hop, same=True):
-        return lax.rem(z + hop, ring) * 2 + (core if same else 1 - core)
-
-    right, left, other = at_chip(1), at_chip(ring - 1), at_chip(0, False)
+    upper = lax.div(z, 2)
+    near_end = z + upper * (last - 2 * z)
+
+    def order(i):
+        base = (near_end, 1 + 2 * near_end, 2 - 2 * near_end, 3 - near_end)[i]
+        return base + upper * (last - 2 * base)
+
+    inner = jnp.logical_and(z >= 1, z <= last - 1)
+    outer = jnp.logical_or(z == 0, z == last)
+    other = (e, z * 2 + 1 - core)
+
+    def at_chip(chip):
+        return (e, chip * 2 + core)
 
     def at_peer(j):
-        return lax.rem(e + j, peers)
+        return (lax.rem(e + j, peers), t)
+
+    sources = [lax.rem(e + peers - j, peers) for j in range(peers)]
+
+    loads = []
+    for i, (src, dst) in enumerate(
+        (
+            (tokens_hbm, tokens_ref), (q_hbm, q_ref), (k_hbm, k_ref), (v_hbm, v_ref),
+            (gate_hbm, gate_ref), (up_hbm, up_ref), (down_hbm, down_ref), (wout_hbm, wout_ref),
+        )
+    ):
+        copy = pltpu.make_async_copy(src, dst, load_sems.at[i])
+        copy.start()
+        loads.append(copy)
 
     barrier = pltpu.get_barrier_semaphore()
-    greeted = [(at_peer(j), t) for j in range(1, peers)] + [(e, right), (e, left), (e, other)]
+    greeted = [at_peer(j) for j in range(1, peers)] + [other]
+    greeted += [at_chip(lax.rem(z + h, chips)) for h in range(1, chips)]
     for device in greeted:
         pl.semaphore_signal(barrier, inc=1, device_id=device, device_id_type=MESH)
+
+    started = []
+
+    def send(src, dst, send_sem, recv_sem, device, when=None):
+        def make():
+            return pltpu.make_async_remote_copy(
+                src_ref=src, dst_ref=dst, send_sem=send_sem, recv_sem=recv_sem,
+                device_id=device, device_id_type=MESH,
+            )
+
+        if when is None:
+            make().start()
+        else:
+            @pl.when(when)
+            def _():
+                make().start()
+        started.append((make, when))
+
+    def arrived(dst, send_sem, recv_sem):
+        pltpu.make_async_remote_copy(
+            src_ref=dst, dst_ref=dst, send_sem=send_sem, recv_sem=recv_sem,
+            device_id=other, device_id_type=MESH,
+        ).wait_recv()
+
+    loads[0].wait()
+    widened = tokens_ref[...].astype(f32)
+    raw[z] = (
+        widened
+        * lax.rsqrt(jnp.mean(widened * widened, axis=-1, keepdims=True) + norm_eps)
+        * scale_ref[...]
+    ).astype(bf16)
+    infos[z] = info_ref[...]
     pl.semaphore_wait(barrier, len(greeted))
 
-    started = []
-
-    def send(src, dst, sems, index, device):
-        copy = pltpu.make_async_remote_copy(
-            src_ref=src,
-            dst_ref=dst,
-            send_sem=sems.at[(0,) + index],
-            recv_sem=sems.at[(1,) + index],
-            device_id=device,
-            device_id_type=MESH,
-        )
-        copy.start()
-        started.append(copy)
-
-    def arrived(dst, sems, index):
-        pltpu.make_async_remote_copy(
-            src_ref=dst,
-            dst_ref=dst,
-            send_sem=sems.at[(0,) + index],
-            recv_sem=sems.at[(1,) + index],
-            device_id=(e, other),
-            device_id_type=MESH,
-        ).wait_recv()
-
-    own = pltpu.make_async_copy(out_ref.at[e], rows.at[t, e], local_sem)
-    own.start()
-    for j in range(1, peers):
-        target = at_peer(j)
-        send(out_ref.at[target], rows.at[t, e], ep_sems, (j,), (target, t))
-    sources = [lax.rem(e + peers - j, peers) for j in range(peers)]
-
-    def piece(hop, j, same=True):
-        return rows.at[at_chip(hop, same), sources[j]]
-
-    def to_other(hop, j):
-        send(piece(hop, j), piece(hop, j), core_sems, (hop, j), (e, other))
-
-    def own_piece(j):
-        if j == 0:
-            own.wait()
+    for n, hop in enumerate((2, -2, 1, -1)):
+        inside = z <= last - hop if hop > 0 else z >= -hop
+        device = at_chip(z + hop)
+        send(infos.at[z], infos.at[z], agi_s.at[n], agi_r.at[z], device, inside)
+        send(raw.at[z], raw.at[z], ag_s.at[n], ag_r.at[z], device, inside)
+
+    def gathered(i):
+        chip = order(i)
+        arrived(infos.at[chip], agi_s.at[0], agi_r.at[chip])
+        arrived(raw.at[chip], ag_s.at[0], ag_r.at[chip])
+
+    def relay():
+        chip = order(1)
+        device = at_chip(last * (z - 1))
+        send(infos.at[chip], infos.at[chip], agi_s.at[4], agi_r.at[chip], device, inner)
+        send(raw.at[chip], raw.at[chip], ag_s.at[4], ag_r.at[chip], device, inner)
+
+    def select(i):
+        chip = order(i)
+        info = infos[chip]
+        goes = info[peers * 8 : peers * 8 + 8]
+        before = lax.broadcasted_iota(jnp.int32, (tokens, tokens), 0) < lax.broadcasted_iota(
+            jnp.int32, (tokens, tokens), 1
+        )
+        rank = jnp.dot(
+            goes.astype(bf16), jnp.where(before, 1.0, 0.0).astype(bf16), preferred_element_type=f32
+        )
+        slot = lax.broadcasted_iota(jnp.int32, (tokens, tokens), 0).astype(f32)
+        for g in range(peers):
+            hit = jnp.logical_and(slot == rank[g : g + 1], goes[g : g + 1] > 0.5)
+            spread = jnp.where(hit, 1.0, 0.0)
+            share = mm(info[g * 8 : g * 8 + 8], spread, ((1,), (1,)))
+            high = share.astype(bf16)
+            low = (share - high.astype(f32)).astype(bf16)
+            stage_share[chip, g] = jnp.concatenate([high, low], axis=0)
+            spreads[chip, g * slots : (g + 1) * slots] = spread[:slots].astype(bf16)
+
+        def columns(n, carry):
+            at = pl.ds(pl.multiple_of(n * 512, 512), 512)
+            picked = jnp.dot(spreads[chip], raw[chip, :, at], preferred_element_type=f32)
+            stage[chip, :, :, at] = picked.astype(bf16).reshape(peers, slots, 512)
+            return carry
+
+        lax.fori_loop(0, width // 512, columns, 0)
+        for j in (3, 1, 2):
+            target = lax.rem(e + j, peers)
+            send(
+                stage_share.at[chip, target], rows_share.at[chip, core, e],
+                eps_s.at[chip, j], eps_r.at[chip, j], (target, t),
+            )
+            send(
+                stage.at[chip, target], rows.at[chip, core, e],
+                ep_s.at[chip, j], ep_r.at[chip, j], (target, t),
+            )
+        rows[chip, core, e] = stage[chip, e]
+        rows_share[chip, core, e] = stage_share[chip, e]
+
+    def pass_on(i):
+        chip = order(i)
+        for j in range(1, peers):
+            arrived(rows_share.at[chip, core, sources[j]], eps_s.at[chip, j], eps_r.at[chip, j])
+            arrived(rows.at[chip, core, sources[j]], ep_s.at[chip, j], ep_r.at[chip, j])
+        send(
+            rows_share.at[chip, core], rows_share.at[chip, core],
+            cores_s.at[chip], cores_r.at[chip], other,
+        )
+        send(rows.at[chip, core], rows.at[chip, core], core_s.at[chip], core_r.at[chip], other)
+
+    def produce(i):
+        chip = order(i)
+        arrived(rows_share.at[chip, 1 - core], cores_s.at[chip], cores_r.at[chip])
+        arrived(rows.at[chip, 1 - core], core_s.at[chip], core_r.at[chip])
+        unit = lax.broadcasted_iota(jnp.int32, (16, 2 * units), 1) // units
+        which = lax.rem(lax.broadcasted_iota(jnp.int32, (16, 2 * units), 0), 8)
+
+        def expert_pair(n, carry):
+            pick = jnp.where(which == unit + 2 * n, 1.0, 0.0).astype(bf16)
+            share = [
+                lax.dot_general(
+                    rows_share[chip, c, p], pick, (((0,), (0,)), ((), ())),
+                    preferred_element_type=f32,
+                )[:slots]
+                for c in range(2)
+                for p in range(peers)
+            ]
+            share = jnp.concatenate(share, axis=0)
+            x = rows[chip].reshape(2 * count, width)
+            gating = lax.dot_general(
+                x, gate_ref[pl.ds(2 * n, 2)].reshape(2 * units, width),
+                (((1,), (1,)), ((), ())), preferred_element_type=f32,
+            )
+            upward = lax.dot_general(
+                x, up_ref[pl.ds(2 * n, 2)].reshape(2 * units, width),
+                (((1,), (1,)), ((), ())), preferred_element_type=f32,
+            )
+            at = pl.ds(pl.multiple_of(n * 2 * units, 2 * units), 2 * units)
+            hid[:, at] = (gating / (1.0 + jnp.exp(-gating)) * upward * share).astype(bf16)
+            return carry
+
+        lax.fori_loop(0, experts // 2, expert_pair, 0)
+
+        def columns(n, carry):
+            at = pl.ds(pl.multiple_of(n * 512, 512), 512)
+            down = down_ref[:, :, at].reshape(experts * units, 512)
+            made = jnp.dot(hid[...], down, preferred_element_type=f32)
+            res[chip, :, :, :, at] = made.astype(bf16).reshape(2, peers, slots, 512)
+            return carry
+
+        lax.fori_loop(0, width // 512, columns, 0)
+        send(res.at[chip, 1 - core], theirs.at[chip], pair_s.at[chip], pair_r.at[chip], other)
+
+    def give_back(i):
+        chip = order(i)
+        arrived(theirs.at[chip], pair_s.at[chip], pair_r.at[chip])
+        res[chip, core] = (res[chip, core].astype(f32) + theirs[chip].astype(f32)).astype(bf16)
+        for j in (3, 1, 2):
+            target = lax.rem(e + j, peers)
+            send(
+                res.at[chip, core, target], back.at[chip, e],
+                back_s.at[chip, j], back_r.at[chip, j], (target, t),
+            )
+        back[chip, e] = res[chip, core, e]
+
+    def unselect(i):
+        chip = order(i)
+        for j in range(1, peers):
+            arrived(back.at[chip, sources[j]], back_s.at[chip, j], back_r.at[chip, j])
+        for h in range(halves):
+            acc[chip, h] = lax.dot_general(
+                spreads[chip],
+                back[chip, :, :, h * half : (h + 1) * half].reshape(count, half),
+                (((0,), (0,)), ((), ())), preferred_element_type=f32,
+            ).astype(bf16)
+
+    def forward(i, when):
+        chip = order(i)
+        way = lax.div(z - chip + last, chips)
+        follows = (1 - way) * z + way * (last - z) > 0
+        following = z + 1 - 2 * way
+        ends = way * (1 - lax.min(lax.abs(following - chip), 1))
+        slot = chip + ends * (chips - chip)
+        for h in range(halves):
+            @pl.when(jnp.logical_and(when, follows))
+            def _():
+                arrived(inb.at[chip, h], rs_s.at[chip, h], rs_r.at[chip, h])
+                acc[chip, h] = (acc[chip, h].astype(f32) + inb[chip, h].astype(f32)).astype(bf16)
+
+            send(
+                acc.at[chip, h], inb.at[slot, h],
+                rs_s.at[chip, h], rs_r.at[slot, h], at_chip(following), when,
+            )
+
+    def finish(first, parts, sems, out, at):
+        @pl.when(z > 0)
+        def _():
+            arrived(parts[0], sems[0], sems[1])
+
+        @pl.when(z < last)
+        def _():
+            arrived(parts[1], sems[0], sems[2])
+
+        @pl.when(z == 0)
+        def _():
+            out[:, at] = (first[...].astype(f32) + parts[1][...].astype(f32)).astype(bf16)
+
+        @pl.when(z == last)
+        def _():
+            out[:, at] = (first[...].astype(f32) + parts[0][...].astype(f32)).astype(bf16)
+
+        @pl.when(inner)
+        def _():
+            total = first[...].astype(f32) + parts[0][...].astype(f32) + parts[1][...].astype(f32)
+            out[:, at] = total.astype(bf16)
+
+    heads = strength_ref.shape[0]
+
+    def send_states():
+        for j in range(1, peers):
+            send(states_out, states_in.at[j], st_s.at[j], st_r.at[j], at_peer(j), e < peers - j)
+
+    def project():
+        state[...] = jnp.zeros_like(state)
+        for j in range(peers - 1, 0, -1):
+            @pl.when(e >= j)
+            def _():
+                arrived(states_in.at[j], st_s.at[j], st_r.at[j])
+                for h in range(heads):
+                    piece = states_in[j, h].astype(f32)
+                    state[h] = piece[:, :DV] + mm(piece[:, DV:], state[h])
+        for h in range(heads):
+            attn[:, h * DV : (h + 1) * DV] = (local[h] + mm(proj[h], state[h])).astype(bf16)
+        loads[7].wait()
+        share = prod.shape[2]
+
+        def columns(n, carry):
+            at = pl.ds(pl.multiple_of(n * 512, 512), 512)
+            made = jnp.dot(attn[...], wout_ref[:, at], preferred_element_type=f32)
+            made = made.astype(bf16).reshape(chips, 2, share, 512)
+            for c in range(2):
+                prod[c, :, :, at] = made[:, c]
+            return carry
+
+        lax.fori_loop(0, width // 512, columns, 0)
+        send(prod.at[1 - core], prod_theirs, pp_s, pp_r, other)
+
+    def join_mixed():
+        arrived(prod_theirs, pp_s, pp_r)
+        prod[core] = (prod[core].astype(f32) + prod_theirs[...].astype(f32)).astype(bf16)
+
+    def mixed_hop(k):
+        for way in range(2):
+            when = z == (k if way == 0 else last - k)
+            targets = range(last, k, -1) if way == 0 else range(0, last - k)
+            for chip in targets:
+                if k > 0:
+                    @pl.when(when)
+                    def _():
+                        arrived(mixed_in.at[chip], mr_s.at[chip], mr_r.at[chip])
+                        prod[core, chip] = (
+                            prod[core, chip].astype(f32) + mixed_in[chip].astype(f32)
+                        ).astype(bf16)
+
+                ends = way == 1 and last - k - 1 == chip
+                slot = chips if ends else chip
+                send(
+                    prod.at[core, chip], mixed_in.at[slot],
+                    mr_s.at[chip], mr_r.at[slot], at_chip(z + 1 - 2 * way), when,
+                )
+
+    select(0)
+    for i in range(1, 4):
+        loads[i].wait()
+    delta_body(q_ref, k_ref, v_ref, strength_ref, decay_ref, local, proj, states_out)
+    send_states()
+    pass_on(0)
+    for i in range(4, 7):
+        loads[i].wait()
+    gathered(1)
+    relay()
+    select(1)
+    produce(0)
+    gathered(2)
+    select(2)
+    project()
+    gathered(3)
+    select(3)
+    join_mixed()
+    mixed_hop(0)
+    pass_on(1)
+    produce(1)
+    give_back(1)
+    mixed_hop(1)
+    pass_on(2)
+    produce(2)
+    mixed_hop(2)
+    pass_on(3)
+    produce(3)
+    give_back(3)
+    give_back(2)
+    give_back(0)
+    finish(
+        prod.at[core, z], (mixed_in.at[z], mixed_in.at[chips]),
+        (mr_s.at[0], mr_r.at[z], mr_r.at[chips]), mixed_ref, slice(0, width),
+    )
+    unselect(1)
+    forward(1, outer)
+    unselect(3)
+    forward(3, outer)
+    forward(1, inner)
+    unselect(2)
+    forward(2, outer)
+    forward(3, inner)
+    forward(2, inner)
+    unselect(0)
+    for h in range(halves):
+        finish(
+            acc.at[z, h], (inb.at[z, h], inb.at[chips, h]),
+            (rs_s.at[0, h], rs_r.at[z, h], rs_r.at[chips, h]),
+            expert_ref, slice(h * half, (h + 1) * half),
+        )
+    for make, when in started:
+        if when is None:
+            make().wait_send()
         else:
-            arrived(piece(0, j), ep_sems, (j,))
-        send(piece(0, j), piece(0, j), near_sems, (0, j), (e, right))
-        send(piece(0, j), piece(0, j), near_sems, (1, j), (e, left))
-        to_other(0, j)
-
-    def near_piece(j):
-        arrived(piece(ring - 1, j), near_sems, (0, j))
-        if j % 2 == 0:
-            send(piece(ring - 1, j), piece(ring - 1, j), far_sems, (j,), (e, right))
-        arrived(piece(1, j), near_sems, (1, j))
-        if j % 2 == 1:
-            send(piece(1, j), piece(1, j), far_sems, (j,), (e, left))
-        to_other(ring - 1, j)
-        to_other(1, j)
-
-    def far_piece(j):
-        arrived(piece(2, j), far_sems, (j,))
-        to_other(2, j)
-
-    def produce(hop):
-        for j in range(peers):
-            arrived(piece(hop, j, False), core_sems, (hop, j))
-
-        def one(k, carry):
-            which = lax.rem(core + 1 + k, 2)
-            block = rows[lax.rem(z + hop, ring) * 2 + which].reshape(peers * slots, -1)
-            x = block[:, :width]
-            hidden = []
-            for n in range(experts):
-                gating = lax.dot_general(
-                    x, gate_ref[n], (((1,), (1,)), ((), ())), preferred_element_type=f32
-                )
-                upward = lax.dot_general(
-                    x, up_ref[n], (((1,), (1,)), ((), ())), preferred_element_type=f32
-                )
-                share = block[:, width + n : width + n + 1].astype(f32) + block[
-                    :, width + experts + n : width + experts + n + 1
-                ].astype(f32)
-                hidden.append((gating / (1.0 + jnp.exp(-gating)) * upward * share).astype(bf16))
-            hidden = jnp.concatenate(hidden, axis=1)
-            down = down_ref[...].reshape(experts * units, width)
-            for h in range(2):
-                part[hop, k, h] = jnp.dot(
-                    hidden, down[:, h * half : (h + 1) * half], preferred_element_type=f32
-                ).astype(bf16)
-            return carry
-
-        lax.fori_loop(0, 2, one, 0)
-        send(part.at[hop, 0], theirs.at[hop], pair_sems, (hop,), (e, other))
-
-    def join(hop):
-        arrived(theirs.at[hop], pair_sems, (hop,))
-        for h in range(2):
-            pair[hop, h] = (part[hop, 1, h].astype(f32) + theirs[hop, h].astype(f32)).astype(bf16)
-
-    for j in range(peers):
-        own_piece(j)
-        if j >= 1:
-            near_piece(j - 1)
-        if j >= 2:
-            far_piece(j - 2)
-    produce(0)
-    near_piece(peers - 1)
-    join(0)
-    far_piece(peers - 2)
-    produce(1)
-    produce(ring - 1)
-    far_piece(peers - 1)
-    join(1)
-    send(pair.at[1, 1], landed.at[0, 1], half_sems, (0, 1), (e, right))
-    join(ring - 1)
-    send(pair.at[ring - 1, 0], landed.at[1, 0], half_sems, (1, 0), (e, left))
-    produce(2)
-    join(2)
-    send(pair.at[2, 0], passed.at[0], half_sems, (2, 0), (e, right))
-    send(pair.at[2, 1], passed.at[1], half_sems, (2, 1), (e, left))
-    arrived(passed.at[0], half_sems, (2, 0))
-    onward[0] = (pair[1, 0].astype(f32) + passed[0].astype(f32)).astype(bf16)
-    send(onward.at[0], landed.at[0, 0], half_sems, (0, 0), (e, right))
-    arrived(passed.at[1], half_sems, (2, 1))
-    onward[1] = (pair[ring - 1, 1].astype(f32) + passed[1].astype(f32)).astype(bf16)
-    send(onward.at[1], landed.at[1, 1], half_sems, (1, 1), (e, left))
-    for h in range(2):
-        arrived(landed.at[h, 1 - h], half_sems, (h, 1 - h))
-    for h in range(2):
-        arrived(landed.at[h, h], half_sems, (h, h))
-        summed = pair[0, h].astype(f32) + landed[0, h].astype(f32) + landed[1, h].astype(f32)
-        total[h] = summed.astype(bf16).reshape(peers, slots, half)
-        for j in range(1, peers):
-            target = at_peer(j)
-            send(total.at[h, target], back.at[h, e], back_sems, (h, j), (target, t))
-        back[h, e] = total[h, e]
-    for h in range(2):
-        for j in range(1, peers):
-            arrived(back.at[h, sources[j]], back_sems, (h, j))
-        result_ref[:, h * half : (h + 1) * half] = jnp.dot(
-            spread_ref[...], back[h].reshape(peers * slots, half), preferred_element_type=f32
-        ).astype(bf16)
-    for copy in started:
-        copy.wait_send()
-
-
-def exchange(outgoing, spread, gate, up, down, ring):
-    peers, slots, wide = outgoing.shape
-    _, _, width = gate.shape
-    count, half = peers * slots, width // 2
-    bf16 = jnp.bfloat16
+            @pl.when(when)
+            def _():
+                make().wait_send()
+
+
+def fused(
+    queries, keys, values, strength, decay_logarithm, out_weight, tokens, scale, info,
+    gate, up, down, slots,
+):
+    experts, units, width = gate.shape
+    count, peers, chips, halves = tokens.shape[0], lax.axis_size("ep"), RING, 2
+    heads, length = strength.shape
+    half = width // halves
+    share = length // (2 * chips)
+    bf16, f32 = jnp.bfloat16, jnp.float32
     vmem = pl.BlockSpec(memory_space=pltpu.VMEM)
+    anywhere = pl.BlockSpec(memory_space=pl.ANY)
     dma = pltpu.SemaphoreType.DMA
-    experts, units, _ = gate.shape
-    total_rows = 2 * ring * count
+
+    def room(*shape, dtype=bf16):
+        return pltpu.VMEM(shape, dtype)
+
+    same = [queries, keys, values, out_weight, tokens, gate, up, down]
     return pl.pallas_call(
-        functools.partial(exchange_kernel, ring),
-        out_shape=jax.ShapeDtypeStruct((spread.shape[0], width), bf16),
-        in_specs=[vmem] * 5,
-        out_specs=vmem,
-        scratch_shapes=[
-            pltpu.VMEM((2 * ring, peers, slots, wide), bf16),
-            pltpu.VMEM((ring, 2, 2, count, half), bf16),
-            pltpu.VMEM((ring, 2, count, half), bf16),
-            pltpu.VMEM((ring, 2, count, half), bf16),
-            pltpu.VMEM((2, count, half), bf16),
-            pltpu.VMEM((2, 2, count, half), bf16),
-            pltpu.VMEM((2, count, half), bf16),
-            pltpu.VMEM((2, peers, slots, half), bf16),
-            pltpu.VMEM((2, peers, slots, half), bf16),
-            dma,
-            dma((2, peers)),
-            dma((2, 2, peers)),
-            dma((2, peers)),
-            dma((2, ring, peers)),
-            dma((2, ring)),
-            dma((2, 3, 2)),
-            dma((2, 2, peers)),
+        fused_kernel,
+        out_shape=(
+            jax.ShapeDtypeStruct((share, width), bf16),
+            jax.ShapeDtypeStruct((count, width), bf16),
+        ),
+        in_specs=[anywhere] * 3 + [vmem] * 2 + [anywhere] * 2 + [vmem] * 2 + [anywhere] * 3,
+        out_specs=(vmem, vmem),
+        scratch_shapes=[room(*a.shape, dtype=a.dtype) for a in same]
+        + [
+            room(chips, count, width),
+            room(chips, *info.shape, dtype=f32),
+            room(chips, peers * slots, count),
+            room(chips, peers, slots, width),
+            room(chips, peers, 16, count),
+            room(chips, 2, peers, slots, width),
+            room(chips, 2, peers, 16, count),
+            room(2 * peers * slots, experts * units),
+            room(chips, 2, peers, slots, width),
+            room(chips, peers, slots, width),
+            room(chips, peers, slots, width),
+            room(chips, halves, count, half),
+            room(chips + 1, halves, count, half),
+            room(heads, length, DV, dtype=f32),
+            room(heads, length, DK, dtype=f32),
+            room(length, heads * DV),
+            room(heads, DK, DV + DK),
+            room(peers, heads, DK, DV + DK),
+            room(heads, DK, DV, dtype=f32),
+            room(2, chips, share, width),
+            room(chips, share, width),
+            room(chips + 1, share, width),
+            dma((8,)),
+            dma((5,)), dma((chips,)), dma((5,)), dma((chips,)),
+            dma((chips, peers)), dma((chips, peers)), dma((chips, peers)), dma((chips, peers)),
+            dma((chips,)), dma((chips,)), dma((chips,)), dma((chips,)),
+            dma((chips,)), dma((chips,)),
+            dma((chips, peers)), dma((chips, peers)),
+            dma((chips, halves)), dma((chips + 1, halves)),
+            dma((peers,)), dma((peers,)), dma, dma,
+            dma((chips,)), dma((chips + 1,)),
         ],
         cost_estimate=pl.CostEstimate(
-            flops=60 * total_rows * experts * units * width,
-            bytes_accessed=6 * experts * units * width,
+            flops=12 * chips * peers * slots * experts * units * width,
+            bytes_accessed=8 * experts * units * width,
             transcendentals=0,
         ),
         compiler_params=pltpu.CompilerParams(
-            collective_id=0, has_side_effects=True, vmem_limit_bytes=60 * 2**20
+            collective_id=0, has_side_effects=True, vmem_limit_bytes=63 * 2**20
         ),
-    )(outgoing, spread, gate, up, down)
+    )(
+        queries, keys, values, strength, decay_logarithm, out_weight, tokens, scale, info,
+        gate, up, down,
+    )
+
+
+def routing(choice, mixing, local_experts, peers):
+    tokens = choice.shape[0]
+    ids, parts = choice.T, mixing.T
+    number = jnp.arange(peers * local_experts, dtype=jnp.int32)[:, None]
+    group = jnp.arange(8, dtype=jnp.int32)[:, None]
+    share = jnp.zeros((peers * local_experts, tokens), jnp.float32)
+    goes = jnp.zeros((8, tokens), bool)
+    for k in range(choice.shape[1]):
+        share = share + jnp.where(ids[k][None] == number, parts[k][None], 0.0)
+        goes = goes | (ids[k][None] // local_experts == group)
+    share = share.reshape(peers, local_experts, tokens)
+    share = jnp.pad(share, ((0, 0), (0, 8 - local_experts), (0, 0))).reshape(peers * 8, tokens)
+    return jnp.concatenate([share, goes.astype(jnp.float32)], axis=0)
 
 
 def by_tokens(normed, choice, mixing, gate, up, down, slots, after):
@@ -408,10 +660,6 @@
     pad = -extra.shape[-1] % 128
     extra = jnp.pad(extra, ((0, 0), (0, 0), (0, pad)))
     outgoing = jnp.concatenate([sent, extra], axis=-1)
-    if lax.axis_size("tp") == 2 * RING and ep_count > 1:
-        outgoing, after = lax.optimization_barrier((outgoing, after))
-        flat = spread.reshape(tokens, ep_count * slots)
-        return exchange(outgoing, flat, gate, up, down, RING), after
     arrived = lax.all_to_all(outgoing, "ep", split_axis=0, concat_axis=0, tiled=True)
     arrived = arrived.reshape(ep_count * slots, -1)
     everyone = lax.all_gather(arrived, "tp", axis=0, tiled=True)
@@ -484,6 +732,25 @@
         * jax.nn.softplus(decay_preactivation.astype(jnp.float32))
         + extra_log_decay
     )
+    leading = jax.nn.sigmoid(expert_logit_difference)
+    mixing = group_router_weight[:, None] * jnp.stack([leading, 1.0 - leading], axis=-1)
+    local_experts, local_units, width = expert_gate_weight.shape
+    own_tokens = second_batch_tokens.shape[0]
+    ep_count, tp_count = lax.axis_size("ep"), lax.axis_size("tp")
+    named_both = TOPK if local_experts % EPG == 0 else 1
+    slots = min(own_tokens, local_experts * CAP // named_both)
+    weights = (expert_gate_weight, expert_up_weight, expert_down_weight)
+    if (
+        (ep_count, tp_count) == (RING, 2 * RING)
+        and named_both == TOPK
+        and own_tokens == DK
+        and local_experts * local_units == width // RING
+    ):
+        return fused(
+            query_heads_rows, key_heads_rows, value_heads_rows, strength, decay_logarithm,
+            output_weight, second_batch_tokens, expert_norm_scale.reshape(1, width),
+            routing(expert_choice_index, mixing, local_experts, ep_count), *weights, slots,
+        )
     local_output, projection_matrix, end_memory = delta_rule(
         query_heads_rows, key_heads_rows, value_heads_rows, strength, decay_logarithm
     )
@@ -504,14 +771,6 @@
         * lax.rsqrt(jnp.mean(widened * widened, axis=-1, keepdims=True) + norm_eps)
         * expert_norm_scale
     ).astype(jnp.bfloat16)
-    leading = jax.nn.sigmoid(expert_logit_difference)
-    mixing = group_router_weight[:, None] * jnp.stack([leading, 1.0 - leading], axis=-1)
-    local_experts, local_units, _ = expert_gate_weight.shape
-    own_tokens = second_batch_tokens.shape[0]
-    ep_count, tp_count = lax.axis_size("ep"), lax.axis_size("tp")
-    named_both = TOPK if local_experts % EPG == 0 else 1
-    slots = min(own_tokens, local_experts * CAP // named_both)
-    weights = (expert_gate_weight, expert_up_weight, expert_down_weight)
     if 2 * tp_count * ep_count * slots < 3 * local_experts * local_units * tp_count:
         expert_out, product = by_tokens(
             normed, expert_choice_index, mixing, *weights, slots, product

time: 253 us -> 134 us (0.53)
  Pallas kernels: 197 us -> 123 us
  waiting for transfers between devices: 25.7 us -> 0 us
  between operations: 14.2 us -> 0.65 us
  matrix products: 7.24 us -> 0 us
    pallas_call x2 -> x1, Pallas kernels: 197 us -> 123 us  [fused(): pl.pallas_call(fused_kernel, out_shape=(jax.ShapeDtypeStruct((share, widt...]
    all_gather x1 -> x0, waiting for transfers between devices: 25.6 us -> none  [incoming(): pieces = lax.all_gather(end_memory, axis)]
    dot_general x8 -> x0, matrix products: 7.24 us -> none  [the longest x3 3.69 us: incoming(): jnp.einsum('hij,hjv->hiv', transfer, state, precision=precise_setting)]
  transfers between devices with their start and end apart: 2 -> 0, of which waited for: 1 -> 0; matrix products, arithmetic and copies ran while one was open for 1% -> 0% of each run, Pallas kernels for 73% -> 0%
where the time goes in v1:
time: 134 us; the launch traced here: 132 us
  Pallas kernels  123 us (92%)
  other arithmetic  4.85 us (4%)
  local copies, waits for them, and re-layouts  3.56 us (3%)
    pallas_call x1, Pallas kernels, fused(): pl.pallas_call(fused_kernel, out_shape=(jax.ShapeDtypeStruct((share, widt...  123 us
    unnamed x2, local copies, waits for them, and re-layouts  3.55 us

profile of v1, /device:TPU:0, one launch (start us, length us, event | category | flops | bytes accessed | tf_op | source)
XLA Modules:
  0.0 131.8 jit_solution(8504379219500826621)
XLA Ops:
  0.6 0.7 exponential_negate_fusion
  1.3 0.7 subtract_bitcast_fusion
  2.0 0.7 fusion.8
  2.6 0.8 slice_bitcast_fusion.3
  3.4 0.1 select_add_fusion
  3.5 1.4 %fusion.5 = (f32[2,512]{1,0:T(2,128)}, f32[2,512]{1,0:T(2,128)}) fusion(f32[2,512]{1,0:T(2,128)} %param.22, bf16[2,512]{1,0:T(2,128)(2,1)} %param.20, f32[2]{0:T(128)S(1)} %exponential_negate_fusion, bf16[2,512]{1,0:T(2,128)(2,1)} %param.19), kind=kLoop, calls=%fused_computation.11 | loop fusion | flops 13312 | bytes 16392 | tf_op jit(solution)/shard_map/add | solution.py:731
  4.9 0.6 pad_maximum_fusion.info_ref
  5.5 122.7 %shard_map.167 = (bf16[64,2048]{1,0:T(8,128)(2,1)}, bf16[128,2048]{1,0:T(8,128)(2,1)}) custom-call(bf16[512,256]{1,0:T(8,128)(2,1)} %q_hbm.1, bf16[512,256]{1,0:T(8,128)(2,1)} %k_hbm.1, bf16[512,256]{1,0:T(8,128)(2,1)} %v_hbm.1, f32[2,512]{1,0:T(2,128)} %get-tuple-element.11.strength_ref, f32[2,512]{1,0:T(2,128)} %get-tuple-element.10.decay_ref, ...), custom_call_target="tpu_custom_call" | custom-call | flops 12884901888 | bytes 8388608 | tf_op jit(solution)/shard_map/pallas_call | solution.py:565
  128.2 1.7 %copy.20 = bf16[64,2048]{1,0:T(8,128)(2,1)} copy(bf16[64,2048]{1,0:T(8,128)(2,1)} %get-tuple-element.14) | data formatting | bytes 524288
  129.9 1.9 %copy.21 = bf16[128,2048]{1,0:T(8,128)(2,1)} copy(bf16[128,2048]{1,0:T(8,128)(2,1)} %get-tuple-element.15) | data formatting | bytes 1048576
  (4 shorter events, 0.0 us)

commit v2 on v1

--- a/solution.py
+++ b/solution.py
@@ -90,6 +90,7 @@
                 inverses[i] = inverses[i] - mm(mm(inverses[i], edge), inverses[i])
         span *= 2
     solved = [mm(inverse, part[2]) for inverse, part in zip(inverses, parts)]
+    yield
     states = [
         jnp.concatenate([jnp.zeros((DK, DV), jnp.float32), eye], axis=1) for _ in range(heads)
     ]
@@ -107,6 +108,12 @@
             proj_ref[h, at, :] = out[:, DV:]
     for h in range(heads):
         end_ref[h] = states[h].astype(end_ref.dtype)
+    yield
+
+
+def delta_kernel(*refs):
+    for _ in delta_body(*refs):
+        pass
 
 
 def delta_rule(queries, keys, values, strength, decay_logarithm):
@@ -114,7 +121,7 @@
     vmem = pl.BlockSpec(memory_space=pltpu.VMEM)
     f32 = jnp.float32
     return pl.pallas_call(
-        delta_body,
+        delta_kernel,
         out_shape=(
             jax.ShapeDtypeStruct((heads, length, DV), f32),
             jax.ShapeDtypeStruct((heads, length, DK), f32),
@@ -168,31 +175,57 @@
     )(rows, gate, up, down)
 
 
-def fused_kernel(
-    q_hbm, k_hbm, v_hbm, strength_ref, decay_ref, wout_hbm, tokens_hbm, scale_ref, info_ref,
-    gate_hbm, up_hbm, down_hbm, mixed_ref, expert_ref,
-    q_ref, k_ref, v_ref, wout_ref, tokens_ref, gate_ref, up_ref, down_ref,
-    raw, infos, spreads, stage, stage_share, rows, rows_share, hid, res, theirs, back,
-    acc, inb, local, proj, attn, states_out, states_in, state, prod, prod_theirs, mixed_in,
-    load_sems, ag_s, ag_r, agi_s, agi_r, ep_s, ep_r, eps_s, eps_r, core_s, core_r, cores_s, cores_r,
-    pair_s, pair_r, back_s, back_r, rs_s, rs_r, st_s, st_r, pp_s, pp_r, mr_s, mr_r,
-):
+def routing(choice, router, difference, experts, peers):
+    tokens = choice.shape[1]
+    f32, i32 = jnp.float32, jnp.int32
+    ids = choice.astype(f32)
+    leading = 1.0 / (1.0 + jnp.exp(-difference))
+    parts = (router * leading, router * (1.0 - leading))
+    line = lax.broadcasted_iota(i32, (peers * 8, tokens), 0)
+    within = lax.rem(line, 8)
+    number = jnp.where(within < experts, line // 8 * experts + within, -1).astype(f32)
+    first = (lax.broadcasted_iota(i32, (8, tokens), 0) * experts).astype(f32)
+    share = jnp.zeros((peers * 8, tokens), f32)
+    goes = jnp.zeros((8, tokens), f32)
+    for k in range(TOPK):
+        named = ids[k : k + 1]
+        share = share + jnp.where(named == number, parts[k], 0.0)
+        inside = jnp.logical_and(named >= first, named < first + experts)
+        goes = jnp.where(inside, 1.0, goes)
+    return jnp.concatenate([share, goes], axis=0)
+
+
+def fused_kernel(*refs):
+    arguments, (mixed_ref, expert_ref), rest = refs[:16], refs[16:18], refs[18:]
+    copies, rest = rest[:16], rest[16:]
+    (
+        tokens_ref, scale_ref, choice_ref, router_ref, difference_ref, logit_ref, before_ref,
+        rate_ref, extra_ref, q_ref, k_ref, v_ref, gate_ref, up_ref, down_ref, wout_ref,
+    ) = copies
+    (
+        raw, infos, spreads, stage, stage_share, rows, rows_share, hid, res, theirs, back,
+        acc, inb, local, proj, attn, states_out, states_in, state, prod, prod_theirs, mixed_in,
+        strength_ref, decay_ref, load_sems, ag_s, ag_r, agi_s, agi_r, ep_s, ep_r, eps_s, eps_r, core_s, core_r, cores_s, cores_r,
+        pair_s, pair_r, back_s, back_r, rs_s, rs_r, st_s, st_r, pp_s, pp_r, mr_s, mr_r,
+    ) = rest
     e, t = lax.axis_index("ep"), lax.axis_index("tp")
     core, z = lax.rem(t, 2), lax.div(t, 2)
     chips, tokens, width = raw.shape
     peers, slots = stage.shape[1], stage.shape[2]
     experts, units, _ = gate_ref.shape
     count = peers * slots
-    halves, half = acc.shape[1], acc.shape[3]
+    pieces, part = acc.shape[1], acc.shape[3]
     last = chips - 1
     bf16, f32 = jnp.bfloat16, jnp.float32
     upper = lax.div(z, 2)
     near_end = z + upper * (last - 2 * z)
 
     def order(i):
-        base = (near_end, 1 + 2 * near_end, 2 - 2 * near_end, 3 - near_end)[i]
+        base = (near_end, 1 + 2 * near_end, 3 - 3 * near_end, 2)[i]
         return base + upper * (last - 2 * base)
 
+    swap = (1 - near_end) * (order(2) - order(1))
+    returns = (order(1) + swap, order(3), order(2) - swap)
     inner = jnp.logical_and(z >= 1, z <= last - 1)
     outer = jnp.logical_or(z == 0, z == last)
     other = (e, z * 2 + 1 - core)
@@ -206,12 +239,7 @@
     sources = [lax.rem(e + peers - j, peers) for j in range(peers)]
 
     loads = []
-    for i, (src, dst) in enumerate(
-        (
-            (tokens_hbm, tokens_ref), (q_hbm, q_ref), (k_hbm, k_ref), (v_hbm, v_ref),
-            (gate_hbm, gate_ref), (up_hbm, up_ref), (down_hbm, down_ref), (wout_hbm, wout_ref),
-        )
-    ):
+    for i, (src, dst) in enumerate(zip(arguments, copies)):
         copy = pltpu.make_async_copy(src, dst, load_sems.at[i])
         copy.start()
         loads.append(copy)
@@ -245,35 +273,35 @@
             device_id=other, device_id_type=MESH,
         ).wait_recv()
 
-    loads[0].wait()
+    for copy in loads[:5]:
+        copy.wait()
     widened = tokens_ref[...].astype(f32)
     raw[z] = (
         widened
         * lax.rsqrt(jnp.mean(widened * widened, axis=-1, keepdims=True) + norm_eps)
         * scale_ref[...]
     ).astype(bf16)
-    infos[z] = info_ref[...]
+    infos[z] = routing(
+        choice_ref[...], router_ref[...], difference_ref[...], experts, peers
+    )
     pl.semaphore_wait(barrier, len(greeted))
 
-    for n, hop in enumerate((2, -2, 1, -1)):
-        inside = z <= last - hop if hop > 0 else z >= -hop
-        device = at_chip(z + hop)
-        send(infos.at[z], infos.at[z], agi_s.at[n], agi_r.at[z], device, inside)
-        send(raw.at[z], raw.at[z], ag_s.at[n], ag_r.at[z], device, inside)
-
-    def gathered(i):
-        chip = order(i)
+    step = 1 - 2 * upper
+
+    def share_rows(n, chip, target, when):
+        device = at_chip(target)
+        send(infos.at[chip], infos.at[chip], agi_s.at[n], agi_r.at[chip], device, when)
+        send(raw.at[chip], raw.at[chip], ag_s.at[n], ag_r.at[chip], device, when)
+
+    share_rows(0, z, z + 2 * step, outer)
+    share_rows(1, z, z + step, outer)
+    share_rows(2, z, z - step, inner)
+
+    def gathered(chip):
         arrived(infos.at[chip], agi_s.at[0], agi_r.at[chip])
         arrived(raw.at[chip], ag_s.at[0], ag_r.at[chip])
 
-    def relay():
-        chip = order(1)
-        device = at_chip(last * (z - 1))
-        send(infos.at[chip], infos.at[chip], agi_s.at[4], agi_r.at[chip], device, inner)
-        send(raw.at[chip], raw.at[chip], ag_s.at[4], ag_r.at[chip], device, inner)
-
-    def select(i):
-        chip = order(i)
+    def select(chip):
         info = infos[chip]
         goes = info[peers * 8 : peers * 8 + 8]
         before = lax.broadcasted_iota(jnp.int32, (tokens, tokens), 0) < lax.broadcasted_iota(
@@ -312,8 +340,7 @@
         rows[chip, core, e] = stage[chip, e]
         rows_share[chip, core, e] = stage_share[chip, e]
 
-    def pass_on(i):
-        chip = order(i)
+    def pass_on(chip):
         for j in range(1, peers):
             arrived(rows_share.at[chip, core, sources[j]], eps_s.at[chip, j], eps_r.at[chip, j])
             arrived(rows.at[chip, core, sources[j]], ep_s.at[chip, j], ep_r.at[chip, j])
@@ -323,8 +350,7 @@
         )
         send(rows.at[chip, core], rows.at[chip, core], core_s.at[chip], core_r.at[chip], other)
 
-    def produce(i):
-        chip = order(i)
+    def produce(chip):
         arrived(rows_share.at[chip, 1 - core], cores_s.at[chip], cores_r.at[chip])
         arrived(rows.at[chip, 1 - core], core_s.at[chip], core_r.at[chip])
         unit = lax.broadcasted_iota(jnp.int32, (16, 2 * units), 1) // units
@@ -366,8 +392,7 @@
         lax.fori_loop(0, width // 512, columns, 0)
         send(res.at[chip, 1 - core], theirs.at[chip], pair_s.at[chip], pair_r.at[chip], other)
 
-    def give_back(i):
-        chip = order(i)
+    def give_back(chip):
         arrived(theirs.at[chip], pair_s.at[chip], pair_r.at[chip])
         res[chip, core] = (res[chip, core].astype(f32) + theirs[chip].astype(f32)).astype(bf16)
         for j in (3, 1, 2):
@@ -378,58 +403,40 @@
             )
         back[chip, e] = res[chip, core, e]
 
-    def unselect(i):
-        chip = order(i)
+    def unselect(chip):
         for j in range(1, peers):
             arrived(back.at[chip, sources[j]], back_s.at[chip, j], back_r.at[chip, j])
-        for h in range(halves):
+        for h in range(pieces):
             acc[chip, h] = lax.dot_general(
                 spreads[chip],
-                back[chip, :, :, h * half : (h + 1) * half].reshape(count, half),
+                back[chip, :, :, h * part : (h + 1) * part].reshape(count, part),
                 (((0,), (0,)), ((), ())), preferred_element_type=f32,
             ).astype(bf16)
 
-    def forward(i, when):
-        chip = order(i)
-        way = lax.div(z - chip + last, chips)
-        follows = (1 - way) * z + way * (last - z) > 0
-        following = z + 1 - 2 * way
-        ends = way * (1 - lax.min(lax.abs(following - chip), 1))
-        slot = chip + ends * (chips - chip)
-        for h in range(halves):
-            @pl.when(jnp.logical_and(when, follows))
-            def _():
-                arrived(inb.at[chip, h], rs_s.at[chip, h], rs_r.at[chip, h])
-                acc[chip, h] = (acc[chip, h].astype(f32) + inb[chip, h].astype(f32)).astype(bf16)
-
-            send(
-                acc.at[chip, h], inb.at[slot, h],
-                rs_s.at[chip, h], rs_r.at[slot, h], at_chip(following), when,
-            )
-
-    def finish(first, parts, sems, out, at):
-        @pl.when(z > 0)
-        def _():
-            arrived(parts[0], sems[0], sems[1])
-
-        @pl.when(z < last)
-        def _():
-            arrived(parts[1], sems[0], sems[2])
-
-        @pl.when(z == 0)
-        def _():
-            out[:, at] = (first[...].astype(f32) + parts[1][...].astype(f32)).astype(bf16)
-
-        @pl.when(z == last)
-        def _():
-            out[:, at] = (first[...].astype(f32) + parts[0][...].astype(f32)).astype(bf16)
-
+    def add_from(total, piece, send_sem, recv_sem):
         @pl.when(inner)
         def _():
-            total = first[...].astype(f32) + parts[0][...].astype(f32) + parts[1][...].astype(f32)
-            out[:, at] = total.astype(bf16)
-
-    heads = strength_ref.shape[0]
+            arrived(piece, send_sem, recv_sem)
+            total[...] = (total[...].astype(f32) + piece[...].astype(f32)).astype(bf16)
+
+    def forward(chip, joins):
+        device = at_chip(chip)
+        if joins:
+            device = at_chip(z + step + near_end * (chip - z - step))
+        slot = chip + (near_end * (chips - chip) if joins else 0)
+        for h in range(pieces):
+            if joins:
+                add_from(acc.at[chip, h], inb.at[chip, h], rs_s.at[chip, h], rs_r.at[chip, h])
+            send(acc.at[chip, h], inb.at[slot, h], rs_s.at[chip, h], rs_r.at[slot, h], device)
+
+    def finish(first, parts, sems, out, at):
+        total = first[...].astype(f32)
+        for piece, sem in zip(parts, sems[1:]):
+            arrived(piece, sems[0], sem)
+            total = total + piece[...].astype(f32)
+        out[:, at] = total.astype(bf16)
+
+    heads = local.shape[0]
 
     def send_states():
         for j in range(1, peers):
@@ -446,7 +453,7 @@
                     state[h] = piece[:, :DV] + mm(piece[:, DV:], state[h])
         for h in range(heads):
             attn[:, h * DV : (h + 1) * DV] = (local[h] + mm(proj[h], state[h])).astype(bf16)
-        loads[7].wait()
+        loads[15].wait()
         share = prod.shape[2]
 
         def columns(n, carry):
@@ -464,76 +471,87 @@
         arrived(prod_theirs, pp_s, pp_r)
         prod[core] = (prod[core].astype(f32) + prod_theirs[...].astype(f32)).astype(bf16)
 
-    def mixed_hop(k):
-        for way in range(2):
-            when = z == (k if way == 0 else last - k)
-            targets = range(last, k, -1) if way == 0 else range(0, last - k)
-            for chip in targets:
-                if k > 0:
-                    @pl.when(when)
-                    def _():
-                        arrived(mixed_in.at[chip], mr_s.at[chip], mr_r.at[chip])
-                        prod[core, chip] = (
-                            prod[core, chip].astype(f32) + mixed_in[chip].astype(f32)
-                        ).astype(bf16)
-
-                ends = way == 1 and last - k - 1 == chip
-                slot = chips if ends else chip
-                send(
-                    prod.at[core, chip], mixed_in.at[slot],
-                    mr_s.at[chip], mr_r.at[slot], at_chip(z + 1 - 2 * way), when,
-                )
-
-    select(0)
-    for i in range(1, 4):
-        loads[i].wait()
-    delta_body(q_ref, k_ref, v_ref, strength_ref, decay_ref, local, proj, states_out)
+    def send_mixed(chip, slot, target, when):
+        send(
+            prod.at[core, chip], mixed_in.at[slot],
+            mr_s.at[chip], mr_r.at[slot], at_chip(target), when,
+        )
+
+    def start_mixed():
+        for n in (3, 2, 1):
+            send_mixed(z + n * step, z + n * step, z + step, outer)
+        send_mixed(z - step, z - step, z - step, inner)
+
+    def pass_mixed():
+        for n in (2, 1):
+            chip = z + n * step
+
+            @pl.when(inner)
+            def _():
+                arrived(mixed_in.at[chip], mr_s.at[chip], mr_r.at[chip])
+                prod[core, chip] = (
+                    prod[core, chip].astype(f32) + mixed_in[chip].astype(f32)
+                ).astype(bf16)
+
+            send_mixed(chip, chips, chip, inner)
+
+    select(order(0))
+    for copy in loads[5:12]:
+        copy.wait()
+    strength_ref[...] = 1.0 / (1.0 + jnp.exp(-logit_ref[...].astype(f32)))
+    before = before_ref[...].astype(f32)
+    growth = jnp.maximum(before, 0.0) + jnp.log1p(jnp.exp(-jnp.abs(before)))
+    for h in range(heads):
+        decay_ref[h : h + 1] = (
+            -jnp.exp(rate_ref[:, h : h + 1]) * growth[h : h + 1] + extra_ref[h : h + 1]
+        )
+    delta = delta_body(q_ref, k_ref, v_ref, strength_ref, decay_ref, local, proj, states_out)
+    next(delta)
+    gathered(order(1))
+    share_rows(3, order(1), z - step, inner)
+    share_rows(1, z, z + step, inner)
+    select(order(1))
+    next(delta)
     send_states()
-    pass_on(0)
-    for i in range(4, 7):
-        loads[i].wait()
-    gathered(1)
-    relay()
-    select(1)
-    produce(0)
-    gathered(2)
-    select(2)
+    pass_on(order(0))
+    for copy in loads[12:15]:
+        copy.wait()
+    produce(order(0))
+    gathered(order(2))
+    share_rows(0, z, z + 2 * step, inner)
+    select(order(2))
+    pass_on(order(1))
+    produce(order(1))
+    gathered(order(3))
+    select(order(3))
     project()
-    gathered(3)
-    select(3)
+    pass_on(order(2))
+    produce(order(2))
     join_mixed()
-    mixed_hop(0)
-    pass_on(1)
-    produce(1)
-    give_back(1)
-    mixed_hop(1)
-    pass_on(2)
-    produce(2)
-    mixed_hop(2)
-    pass_on(3)
-    produce(3)
-    give_back(3)
-    give_back(2)
-    give_back(0)
+    start_mixed()
+    give_back(returns[0])
+    pass_on(order(3))
+    produce(order(3))
+    give_back(returns[1])
+    give_back(returns[2])
+    give_back(order(0))
+    pass_mixed()
+    unselect(returns[0])
+    forward(returns[0], True)
+    unselect(returns[1])
+    forward(returns[1], True)
     finish(
         prod.at[core, z], (mixed_in.at[z], mixed_in.at[chips]),
         (mr_s.at[0], mr_r.at[z], mr_r.at[chips]), mixed_ref, slice(0, width),
     )
-    unselect(1)
-    forward(1, outer)
-    unselect(3)
-    forward(3, outer)
-    forward(1, inner)
-    unselect(2)
-    forward(2, outer)
-    forward(3, inner)
-    forward(2, inner)
-    unselect(0)
-    for h in range(halves):
+    unselect(returns[2])
+    forward(returns[2], False)
+    unselect(order(0))
+    for h in range(pieces):
         finish(
             acc.at[z, h], (inb.at[z, h], inb.at[chips, h]),
             (rs_s.at[0, h], rs_r.at[z, h], rs_r.at[chips, h]),
-            expert_ref, slice(h * half, (h + 1) * half),
+            expert_ref, slice(h * part, (h + 1) * part),
         )
     for make, when in started:
         if when is None:
@@ -545,13 +563,13 @@
 
 
 def fused(
-    queries, keys, values, strength, decay_logarithm, out_weight, tokens, scale, info,
-    gate, up, down, slots,
+    tokens, scale, choice, router, difference, logit, before, rate, extra,
+    queries, keys, values, gate, up, down, out_weight, slots,
 ):
     experts, units, width = gate.shape
-    count, peers, chips, halves = tokens.shape[0], lax.axis_size("ep"), RING, 2
-    heads, length = strength.shape
-    half = width // halves
+    count, peers, chips, pieces = tokens.shape[0], lax.axis_size("ep"), RING, 4
+    heads, length = extra.shape
+    part = width // pieces
     share = length // (2 * chips)
     bf16, f32 = jnp.bfloat16, jnp.float32
     vmem = pl.BlockSpec(memory_space=pltpu.VMEM)
@@ -561,19 +579,22 @@
     def room(*shape, dtype=bf16):
         return pltpu.VMEM(shape, dtype)
 
-    same = [queries, keys, values, out_weight, tokens, gate, up, down]
+    arguments = [
+        tokens, scale, choice, router, difference, logit, before, rate, extra,
+        queries, keys, values, gate, up, down, out_weight,
+    ]
     return pl.pallas_call(
         fused_kernel,
         out_shape=(
             jax.ShapeDtypeStruct((share, width), bf16),
             jax.ShapeDtypeStruct((count, width), bf16),
         ),
-        in_specs=[anywhere] * 3 + [vmem] * 2 + [anywhere] * 2 + [vmem] * 2 + [anywhere] * 3,
+        in_specs=[anywhere] * len(arguments),
         out_specs=(vmem, vmem),
-        scratch_shapes=[room(*a.shape, dtype=a.dtype) for a in same]
+        scratch_shapes=[room(*a.shape, dtype=a.dtype) for a in arguments]
         + [
             room(chips, count, width),
-            room(chips, *info.shape, dtype=f32),
+            room(chips, (peers + 1) * 8, count, dtype=f32),
             room(chips, peers * slots, count),
             room(chips, peers, slots, width),
             room(chips, peers, 16, count),
@@ -583,8 +604,8 @@
             room(chips, 2, peers, slots, width),
             room(chips, peers, slots, width),
             room(chips, peers, slots, width),
-            room(chips, halves, count, half),
-            room(chips + 1, halves, count, half),
+            room(chips, pieces, count, part),
+            room(chips + 1, pieces, count, part),
             room(heads, length, DV, dtype=f32),
             room(heads, length, DK, dtype=f32),
             room(length, heads * DV),
@@ -594,13 +615,15 @@
             room(2, chips, share, width),
             room(chips, share, width),
             room(chips + 1, share, width),
-            dma((8,)),
+            room(heads, length, dtype=f32),
+            room(heads, length, dtype=f32),
+            dma((len(arguments),)),
             dma((5,)), dma((chips,)), dma((5,)), dma((chips,)),
             dma((chips, peers)), dma((chips, peers)), dma((chips, peers)), dma((chips, peers)),
             dma((chips,)), dma((chips,)), dma((chips,)), dma((chips,)),
             dma((chips,)), dma((chips,)),
             dma((chips, peers)), dma((chips, peers)),
-            dma((chips, halves)), dma((chips + 1, halves)),
+            dma((chips, pieces)), dma((chips + 1, pieces)),
             dma((peers,)), dma((peers,)), dma, dma,
             dma((chips,)), dma((chips + 1,)),
         ],
@@ -612,25 +635,7 @@
         compiler_params=pltpu.CompilerParams(
             collective_id=0, has_side_effects=True, vmem_limit_bytes=63 * 2**20
         ),
-    )(
-        queries, keys, values, strength, decay_logarithm, out_weight, tokens, scale, info,
-        gate, up, down,
-    )
-
-
-def routing(choice, mixing, local_experts, peers):
-    tokens = choice.shape[0]
-    ids, parts = choice.T, mixing.T
-    number = jnp.arange(peers * local_experts, dtype=jnp.int32)[:, None]
-    group = jnp.arange(8, dtype=jnp.int32)[:, None]
-    share = jnp.zeros((peers * local_experts, tokens), jnp.float32)
-    goes = jnp.zeros((8, tokens), bool)
-    for k in range(choice.shape[1]):
-        share = share + jnp.where(ids[k][None] == number, parts[k][None], 0.0)
-        goes = goes | (ids[k][None] // local_experts == group)
-    share = share.reshape(peers, local_experts, tokens)
-    share = jnp.pad(share, ((0, 0), (0, 8 - local_experts), (0, 0))).reshape(peers * 8, tokens)
-    return jnp.concatenate([share, goes.astype(jnp.float32)], axis=0)
+    )(*arguments)
 
 
 def by_tokens(normed, choice, mixing, gate, up, down, slots, after):
@@ -747,9 +752,12 @@
         and local_experts * local_units == width // RING
     ):
         return fused(
-            query_heads_rows, key_heads_rows, value_heads_rows, strength, decay_logarithm,
-            output_weight, second_batch_tokens, expert_norm_scale.reshape(1, width),
-            routing(expert_choice_index, mixing, local_experts, ep_count), *weights, slots,
+            second_batch_tokens, expert_norm_scale.reshape(1, width), expert_choice_index.T,
+            group_router_weight.reshape(1, own_tokens),
+            expert_logit_difference.reshape(1, own_tokens),
+            write_strength_logit, decay_preactivation,
+            head_decay_logarithm.reshape(1, local_heads), extra_log_decay,
+            query_heads_rows, key_heads_rows, value_heads_rows, *weights, output_weight, slots,
         )
     local_output, projection_matrix, end_memory = delta_rule(
         query_heads_rows, key_heads_rows, value_heads_rows, strength, decay_logarithm

time: 134 us -> 121 us (0.903); the launches traced: 132 us -> 121 us
  Pallas kernels: 123 us -> 117 us
  other arithmetic: 4.85 us -> 0 us
    pallas_call x1, Pallas kernels: 123 us -> 117 us  [fused(): pl.pallas_call(fused_kernel, out_shape=(jax.ShapeDtypeStruct((share, widt...]
    add x2 -> x0, other arithmetic: 1.46 us -> none  [the longest x1 1.38 us: shards(): -jnp.exp(head_decay_logarithm)[:, None]]
where the time goes in v2:
time: 121 us
  Pallas kernels  117 us (97%)
  local copies, waits for them, and re-layouts  3.55 us (3%)
    pallas_call x1, Pallas kernels, fused(): pl.pallas_call(fused_kernel, out_shape=(jax.ShapeDtypeStruct((share, widt...  117 us
    unnamed x2, local copies, waits for them, and re-layouts  3.55 us

profile of v2, /device:TPU:0, one launch (start us, length us, event | category | flops | bytes accessed | tf_op | source)
XLA Modules:
  0.0 121.3 jit_solution(7404682471785898950)
XLA Ops:
  0.6 117.1 %shard_map.167 = (bf16[64,2048]{1,0:T(8,128)(2,1)}, bf16[128,2048]{1,0:T(8,128)(2,1)}) custom-call(bf16[128,2048]{1,0:T(8,128)(2,1)} %refs_0_.1, f32[1,2048]{1,0:T(1,128)} %bitcast.5, s32[2,128]{1,0:T(2,128)} %bitcast.6, f32[1,128]{1,0:T(1,128)} %bitcast.7, f32[1,128]{1,0:T(1,128)} %bitcast.8, bf16[2,512]{1,0:T(2,128)(2,1)} %refs_5_.1, ...), custom_call_target="tpu_custom_call" | custom-call | flops 12884901888 | bytes 8388608 | tf_op jit(solution)/shard_map/pallas_call | solution.py:586
  117.7 1.7 %copy.20 = bf16[64,2048]{1,0:T(8,128)(2,1)} copy(bf16[64,2048]{1,0:T(8,128)(2,1)} %get-tuple-element.4) | data formatting | bytes 524288
  119.4 1.9 %copy.21 = bf16[128,2048]{1,0:T(8,128)(2,1)} copy(bf16[128,2048]{1,0:T(8,128)(2,1)} %get-tuple-element.5) | data formatting | bytes 1048576

commit v3 on v2

--- a/solution.py
+++ b/solution.py
@@ -419,15 +419,22 @@
             arrived(piece, send_sem, recv_sem)
             total[...] = (total[...].astype(f32) + piece[...].astype(f32)).astype(bf16)
 
-    def forward(chip, joins):
-        device = at_chip(chip)
-        if joins:
-            device = at_chip(z + step + near_end * (chip - z - step))
+    def forward(chip, joins, which, when=None):
+        device = at_chip(z + step + near_end * (chip - z - step))
         slot = chip + (near_end * (chips - chip) if joins else 0)
-        for h in range(pieces):
+        for h in which:
             if joins:
                 add_from(acc.at[chip, h], inb.at[chip, h], rs_s.at[chip, h], rs_r.at[chip, h])
-            send(acc.at[chip, h], inb.at[slot, h], rs_s.at[chip, h], rs_r.at[slot, h], device)
+            send(
+                acc.at[chip, h], inb.at[slot, h], rs_s.at[chip, h], rs_r.at[slot, h], device, when
+            )
+
+    def keep_order():
+        def body(i, carry):
+            state[0] = jnp.zeros_like(state[0])
+            return carry
+
+        lax.fori_loop(0, t // (4 * chips), body, 0)
 
     def finish(first, parts, sems, out, at):
         total = first[...].astype(f32)
@@ -496,6 +503,7 @@
             send_mixed(chip, chips, chip, inner)
 
     select(order(0))
+    keep_order()
     for copy in loads[5:12]:
         copy.wait()
     strength_ref[...] = 1.0 / (1.0 + jnp.exp(-logit_ref[...].astype(f32)))
@@ -507,46 +515,75 @@
         )
     delta = delta_body(q_ref, k_ref, v_ref, strength_ref, decay_ref, local, proj, states_out)
     next(delta)
+    keep_order()
     gathered(order(1))
     share_rows(3, order(1), z - step, inner)
     share_rows(1, z, z + step, inner)
     select(order(1))
+    keep_order()
     next(delta)
+    keep_order()
     send_states()
     pass_on(order(0))
+    keep_order()
     for copy in loads[12:15]:
         copy.wait()
     produce(order(0))
+    keep_order()
     gathered(order(2))
     share_rows(0, z, z + 2 * step, inner)
     select(order(2))
+    keep_order()
     pass_on(order(1))
+    keep_order()
     produce(order(1))
+    keep_order()
     gathered(order(3))
     select(order(3))
+    keep_order()
     project()
+    keep_order()
     pass_on(order(2))
+    keep_order()
     produce(order(2))
+    keep_order()
     join_mixed()
     start_mixed()
+    keep_order()
     give_back(returns[0])
+    keep_order()
     pass_on(order(3))
+    keep_order()
     produce(order(3))
+    keep_order()
     give_back(returns[1])
+    keep_order()
     give_back(returns[2])
+    keep_order()
     give_back(order(0))
+    keep_order()
     pass_mixed()
+    keep_order()
     unselect(returns[0])
-    forward(returns[0], True)
+    keep_order()
+    forward(returns[0], True, range(pieces))
+    keep_order()
     unselect(returns[1])
-    forward(returns[1], True)
+    keep_order()
+    forward(returns[1], False, range(pieces), outer)
+    forward(returns[1], True, range(pieces // 2), inner)
+    keep_order()
     finish(
         prod.at[core, z], (mixed_in.at[z], mixed_in.at[chips]),
         (mr_s.at[0], mr_r.at[z], mr_r.at[chips]), mixed_ref, slice(0, width),
     )
     unselect(returns[2])
-    forward(returns[2], False)
+    keep_order()
+    forward(returns[2], False, range(pieces))
+    forward(returns[1], True, range(pieces // 2, pieces), inner)
+    keep_order()
     unselect(order(0))
+    keep_order()
     for h in range(pieces):
         finish(
             acc.at[z, h], (inb.at[z, h], inb.at[chips, h]),

time: 121 us -> 117 us (0.967)
  Pallas kernels: 117 us -> 113 us
    pallas_call x1, Pallas kernels: 117 us -> 113 us  [fused(): pl.pallas_call(fused_kernel, out_shape=(jax.ShapeDtypeStruct((share, widt...]
where the time goes in v3:
time: 117 us
  Pallas kernels  113 us (97%)
  local copies, waits for them, and re-layouts  3.55 us (3%)
    pallas_call x1, Pallas kernels, fused(): pl.pallas_call(fused_kernel, out_shape=(jax.ShapeDtypeStruct((share, widt...  113 us
    unnamed x2, local copies, waits for them, and re-layouts  3.55 us

profile of v3, /device:TPU:0, one launch (start us, length us, event | category | flops | bytes accessed | tf_op | source)
XLA Modules:
  0.0 117.2 jit_solution(4364449387079855254)
XLA Ops:
  0.6 113.0 %shard_map.167 = (bf16[64,2048]{1,0:T(8,128)(2,1)}, bf16[128,2048]{1,0:T(8,128)(2,1)}) custom-call(bf16[128,2048]{1,0:T(8,128)(2,1)} %refs_0_.1, f32[1,2048]{1,0:T(1,128)} %bitcast.5, s32[2,128]{1,0:T(2,128)} %bitcast.6, f32[1,128]{1,0:T(1,128)} %bitcast.7, f32[1,128]{1,0:T(1,128)} %bitcast.8, bf16[2,512]{1,0:T(2,128)(2,1)} %refs_5_.1, ...), custom_call_target="tpu_custom_call" | custom-call | flops 12884901888 | bytes 8388608 | tf_op jit(solution)/shard_map/pallas_call | solution.py:623
  113.6 1.7 %copy.20 = bf16[64,2048]{1,0:T(8,128)(2,1)} copy(bf16[64,2048]{1,0:T(8,128)(2,1)} %get-tuple-element.4) | data formatting | bytes 524288
  115.3 1.9 %copy.21 = bf16[128,2048]{1,0:T(8,128)(2,1)} copy(bf16[128,2048]{1,0:T(8,128)(2,1)} %get-tuple-element.5) | data formatting | bytes 1048576

commit v4 on v3

--- a/solution.py
+++ b/solution.py
@@ -196,7 +196,7 @@
 
 
 def fused_kernel(*refs):
-    arguments, (mixed_ref, expert_ref), rest = refs[:16], refs[16:18], refs[18:]
+    arguments, (mixed_hbm, expert_hbm), rest = refs[:16], refs[16:18], refs[18:]
     copies, rest = rest[:16], rest[16:]
     (
         tokens_ref, scale_ref, choice_ref, router_ref, difference_ref, logit_ref, before_ref,
@@ -205,7 +205,7 @@
     (
         raw, infos, spreads, stage, stage_share, rows, rows_share, hid, res, theirs, back,
         acc, inb, local, proj, attn, states_out, states_in, state, prod, prod_theirs, mixed_in,
-        strength_ref, decay_ref, load_sems, ag_s, ag_r, agi_s, agi_r, ep_s, ep_r, eps_s, eps_r, core_s, core_r, cores_s, cores_r,
+        strength_ref, decay_ref, mixed_ref, expert_ref, load_sems, out_sems, ag_s, ag_r, agi_s, agi_r, ep_s, ep_r, eps_s, eps_r, core_s, core_r, cores_s, cores_r,
         pair_s, pair_r, back_s, back_r, rs_s, rs_r, st_s, st_r, pp_s, pp_r, mr_s, mr_r,
     ) = rest
     e, t = lax.axis_index("ep"), lax.axis_index("tp")
@@ -436,12 +436,17 @@
 
         lax.fori_loop(0, t // (4 * chips), body, 0)
 
-    def finish(first, parts, sems, out, at):
+    written = []
+
+    def finish(first, parts, sems, out, target, at):
         total = first[...].astype(f32)
         for piece, sem in zip(parts, sems[1:]):
             arrived(piece, sems[0], sem)
             total = total + piece[...].astype(f32)
-        out[:, at] = total.astype(bf16)
+        out[...] = total.astype(bf16)
+        copy = pltpu.make_async_copy(out, target.at[:, at], out_sems.at[len(written)])
+        copy.start()
+        written.append(copy)
 
     heads = local.shape[0]
 
@@ -575,7 +580,7 @@
     keep_order()
     finish(
         prod.at[core, z], (mixed_in.at[z], mixed_in.at[chips]),
-        (mr_s.at[0], mr_r.at[z], mr_r.at[chips]), mixed_ref, slice(0, width),
+        (mr_s.at[0], mr_r.at[z], mr_r.at[chips]), mixed_ref, mixed_hbm, pl.ds(0, width),
     )
     unselect(returns[2])
     keep_order()
@@ -588,8 +593,10 @@
         finish(
             acc.at[z, h], (inb.at[z, h], inb.at[chips, h]),
             (rs_s.at[0, h], rs_r.at[z, h], rs_r.at[chips, h]),
-            expert_ref, slice(h * part, (h + 1) * part),
-        )
+            expert_ref.at[h], expert_hbm, pl.ds(h * part, part),
+        )
+    for copy in written:
+        copy.wait()
     for make, when in started:
         if when is None:
             make().wait_send()
@@ -597,6 +604,42 @@
             @pl.when(when)
             def _():
                 make().wait_send()
+
+
+def hand_over_kernel(first, second, first_out, second_out, held, in_sems, out_sems):
+    block = held.shape[1]
+    moves = []
+    for source, target in ((first, first_out), (second, second_out)):
+        for n in range(source.shape[0] // block):
+            at = pl.ds(n * block, block)
+            i = len(moves)
+            read = pltpu.make_async_copy(source.at[at], held.at[i], in_sems.at[i])
+            write = pltpu.make_async_copy(held.at[i], target.at[at], out_sems.at[i])
+            read.start()
+            moves.append((read, write))
+    for read, write in moves:
+        read.wait()
+        write.start()
+    for read, write in moves:
+        write.wait()
+
+
+def hand_over(first, second):
+    block = first.shape[0] // 2
+    count = (first.shape[0] + second.shape[0]) // block
+    anywhere = pl.BlockSpec(memory_space=pl.ANY)
+    return pl.pallas_call(
+        hand_over_kernel,
+        out_shape=tuple(jax.ShapeDtypeStruct(a.shape, a.dtype) for a in (first, second)),
+        in_specs=[anywhere] * 2,
+        out_specs=(anywhere, anywhere),
+        scratch_shapes=[
+            pltpu.VMEM((count, block, first.shape[1]), first.dtype),
+            pltpu.SemaphoreType.DMA((count,)),
+            pltpu.SemaphoreType.DMA((count,)),
+        ],
+        compiler_params=pltpu.CompilerParams(vmem_limit_bytes=67043328),
+    )(first, second)
 
 
 def fused(
@@ -609,7 +652,6 @@
     part = width // pieces
     share = length // (2 * chips)
     bf16, f32 = jnp.bfloat16, jnp.float32
-    vmem = pl.BlockSpec(memory_space=pltpu.VMEM)
     anywhere = pl.BlockSpec(memory_space=pl.ANY)
     dma = pltpu.SemaphoreType.DMA
 
@@ -620,14 +662,14 @@
         tokens, scale, choice, router, difference, logit, before, rate, extra,
         queries, keys, values, gate, up, down, out_weight,
     ]
-    return pl.pallas_call(
+    mixed, expert = pl.pallas_call(
         fused_kernel,
         out_shape=(
             jax.ShapeDtypeStruct((share, width), bf16),
             jax.ShapeDtypeStruct((count, width), bf16),
         ),
         in_specs=[anywhere] * len(arguments),
-        out_specs=(vmem, vmem),
+        out_specs=(anywhere, anywhere),
         scratch_shapes=[room(*a.shape, dtype=a.dtype) for a in arguments]
         + [
             room(chips, count, width),
@@ -654,7 +696,9 @@
             room(chips + 1, share, width),
             room(heads, length, dtype=f32),
             room(heads, length, dtype=f32),
-            dma((len(arguments),)),
+            room(share, width),
+            room(pieces, count, part),
+            dma((len(arguments),)), dma((1 + pieces,)),
             dma((5,)), dma((chips,)), dma((5,)), dma((chips,)),
             dma((chips, peers)), dma((chips, peers)), dma((chips, peers)), dma((chips, peers)),
             dma((chips,)), dma((chips,)), dma((chips,)), dma((chips,)),
@@ -673,6 +717,7 @@
             collective_id=0, has_side_effects=True, vmem_limit_bytes=63 * 2**20
         ),
     )(*arguments)
+    return hand_over(mixed, expert)
 
 
 def by_tokens(normed, choice, mixing, gate, up, down, slots, after):

time: 117 us -> 116 us (level)
  local copies, waits for them, and re-layouts: 3.55 us -> 0 us
  Pallas kernels: 113 us -> 115 us
    unnamed x2 -> x0, local copies, waits for them, and re-layouts: 3.55 us -> none
    pallas_call x0 -> x1, Pallas kernels: none -> 1.97 us  [hand_over(): pl.pallas_call(hand_over_kernel, out_shape=tuple((jax.ShapeDtypeStruct(a....]
where the time goes in v4:
time: 116 us
  Pallas kernels  115 us (99%)
    pallas_call x1, Pallas kernels, fused(): pl.pallas_call(fused_kernel, out_shape=(jax.ShapeDtypeStruct((share, widt...  113 us

profile of v4, /device:TPU:0, one launch (start us, length us, event | category | flops | bytes accessed | tf_op | source)
XLA Modules:
  0.0 115.6 jit_solution(9406118773084932010)
XLA Ops:
  0.6 112.8 %shard_map.167 = (bf16[64,2048]{1,0:T(8,128)(2,1)}, bf16[128,2048]{1,0:T(8,128)(2,1)}) custom-call(bf16[128,2048]{1,0:T(8,128)(2,1)} %refs_0_.1, f32[1,2048]{1,0:T(1,128)} %bitcast.5, s32[2,128]{1,0:T(2,128)} %bitcast.6, f32[1,128]{1,0:T(1,128)} %bitcast.7, f32[1,128]{1,0:T(1,128)} %bitcast.8, bf16[2,512]{1,0:T(2,128)(2,1)} %refs_5_.1, ...), custom_call_target="tpu_custom_call" | custom-call | flops 12884901888 | bytes 8388608 | tf_op jit(solution)/shard_map/pallas_call | solution.py:665
  113.5 2.0 %shard_map.168 = (bf16[64,2048]{1,0:T(8,128)(2,1)}, bf16[128,2048]{1,0:T(8,128)(2,1)}) custom-call(bf16[64,2048]{1,0:T(8,128)(2,1)} %get-tuple-element.4.first, bf16[128,2048]{1,0:T(8,128)(2,1)} %get-tuple-element.5.second), custom_call_target="tpu_custom_call" | custom-call | tf_op jit(solution)/shard_map/pallas_call | solution.py:631
